TPU v7x, 32 devices: a whole 2x2x4 slice. The times are simulated.
32 devices in a mesh: sp: 4 (over z), fs: 4 (over y, x), tp: 2 (over core).
Axes of the slice: x: 2, y: 2, z: 4, core: 2. Of those that a mesh axis runs over, the one named last changes fastest.
Arguments:
- tokens: bfloat16 [4, 768, 2048], P('fs', 'sp', 'tp'), may hold values from -24 to 24
- norm_gain: bfloat16 [2048], P('tp'), may hold values from 0.099609375 to 1.8984375
- w_q_down: bfloat16 [2048, 512], P('fs'), may hold values from -0.151 to 0.151
- q_gain: float32 [512], replicated, may hold values from 0.1 to 1.9
- w_q_nope: bfloat16 [512, 2048], P(None, 'tp'), may hold values from -1.21 to 1.21
- w_q_rope: bfloat16 [512, 1024], P(None, 'tp'), may hold values from -0.75 to 0.75
- w_kv_down: bfloat16 [2048, 256], P('fs'), may hold values from -0.151 to 0.151
- kv_gain: float32 [256], replicated, may hold values from 0.1 to 1.9
- w_k_up: bfloat16 [256, 2048], P(None, 'tp'), may hold values from -0.81 to 0.81
- w_v_up: bfloat16 [256, 2048], P(None, 'tp'), may hold values from -0.375 to 0.375
- w_k_rope: bfloat16 [2048, 64], replicated, may hold values from -0.125 to 0.125
- w_pool_in: bfloat16 [2048, 1024], P(None, 'tp'), may hold values from -0.125 to 0.125
- w_pool_mix: bfloat16 [4, 256, 256], replicated, may hold values from -0.375 to 0.375
- w_out_attn: bfloat16 [2048, 2048], P('tp'), may hold values from -0.125 to 0.125
- w_out_pool: bfloat16 [1024, 2048], P('tp'), may hold values from -0.1875 to 0.1875
Outputs:
- mixed: bfloat16 [4, 768, 2048], P('fs', ('sp', 'tp'))
All inputs are finite; a program needn't handle non-finite values.
Results may differ from a plain program's by a relative error of at most 0.02.
Values may be sent and summed in bfloat16 or wider, within the bound.
A program may use at most 128 MiB of HBM per device.

v0:
```python
import functools
import math

import jax
import jax.numpy as jnp
from jax import lax
from jax.experimental import pallas as pl
from jax.experimental.pallas import tpu as pltpu
from jax.sharding import PartitionSpec as P

NOPE_DIM = 128
ROPE_DIM = 64
VALUE_DIM = 128
GRID_W = 64
POOL_GROUP = 256
EPS = 1e-06
THETA = 10000.0
WINDOWS = (2, 4, 8, 16)
RIM = 8
SPAN_LIMIT = 1024
F32 = jnp.float32
BF16 = jnp.bfloat16
MESH = pl.DeviceIdType.MESH


def mm(a, b):
    return jnp.dot(a, b, preferred_element_type=F32)


def mm_t(a, b):
    return lax.dot_general(a, b, (((1,), (1,)), ((), ())), preferred_element_type=F32)


def normed(wide, gain):
    scale = lax.rsqrt(jnp.mean(wide * wide, axis=-1, keepdims=True) + EPS)
    return (wide * scale * gain).astype(BF16)


def layer(
    n_sp,
    n_fs,
    tokens,
    norm_gain,
    w_q_down,
    q_gain,
    w_q_nope,
    w_q_rope,
    w_kv_down,
    kv_gain,
    w_k_up,
    w_v_up,
    w_k_rope,
    w_pool_in,
    w_pool_mix,
    w_out_attn,
    w_out_pool,
    out,
    tok,
    gain,
    hid,
    wq_all,
    wkv_all,
    qg,
    kvg,
    wqn,
    wqr,
    wku,
    wvu,
    wkr,
    wpi,
    mix,
    woa,
    wop,
    halo_out,
    halo_in,
    kvp,
    qp,
    ropes,
    kcat,
    qcat,
    ctx,
    att,
    acc,
    share,
    arrived,
    local_sem,
    send_sem,
    recv_sem,
    gather_send,
    gather_recv,
    pass_send,
    pass_recv,
    rope_send,
    rope_recv,
):
    s = lax.axis_index("sp")
    f = lax.axis_index("fs")
    t = lax.axis_index("tp")
    rows = tok.shape[1]
    half = rows // 2
    depth = w_q_down.shape[0]
    q_half = wq_all.shape[1]
    kv_half = wkv_all.shape[1]
    kv_rank = 2 * kv_half
    heads = wqn.shape[1] // NOPE_DIM
    groups = wpi.shape[1] // POOL_GROUP
    length = rows * n_sp

    def col(ref, width):
        return ref.at[:, pl.ds(pl.multiple_of(t * width, width), width)]

    def down(ref, owner, first=0, size=depth):
        start = pl.multiple_of(owner * depth + first, 16)
        return ref.at[pl.ds(start, size), :]

    pairs = (
        (tokens.at[0], tok.at[t]),
        (norm_gain, gain.at[t]),
        (col(w_kv_down, kv_half), down(wkv_all, f)),
        (col(w_q_down, q_half), down(wq_all, f)),
        (w_k_rope, wkr),
        (w_pool_in, wpi),
        (kv_gain, kvg),
        (q_gain, qg),
        (w_pool_mix.at[pl.ds(t * groups, groups)], mix),
        (w_out_pool, wop),
        (w_q_nope, wqn),
        (w_q_rope, wqr),
        (w_k_up, wku),
        (w_v_up, wvu),
        (w_out_attn, woa),
    )
    loads = [
        pltpu.make_async_copy(src, dst, local_sem.at[i]) for i, (src, dst) in enumerate(pairs)
    ]
    for load in loads:
        load.start()
    (
        l_tok,
        l_gain,
        l_kv,
        l_q,
        l_kr,
        l_pi,
        l_kvg,
        l_qg,
        l_mix,
        l_op,
        l_qn,
        l_qr,
        l_ku,
        l_vu,
        l_oa,
    ) = loads

    def signal_all():
        barrier = pltpu.get_barrier_semaphore()
        pl.semaphore_signal(barrier, inc=1, device_id={"tp": 1 - t}, device_id_type=MESH)
        for j in range(1, n_fs):
            pl.semaphore_signal(
                barrier, inc=1, device_id={"fs": (f + j) % n_fs}, device_id_type=MESH
            )
        for j in range(1, n_sp):
            pl.semaphore_signal(
                barrier, inc=1, device_id={"sp": (s + j) % n_sp}, device_id_type=MESH
            )
        return barrier

    barrier = signal_all()

    lane = lax.broadcasted_iota(jnp.int32, (rows, 128), 1)
    place = s * rows + lax.broadcasted_iota(jnp.int32, (rows, 128), 0)
    quarter = ROPE_DIM // 4
    power = (lane % quarter).astype(F32) * (2.0 / (ROPE_DIM // 2))
    inverse = jnp.exp(power * (-math.log(THETA)))
    grid_row = place // GRID_W
    grid_col = place - grid_row * GRID_W
    in_a = (lane % ROPE_DIM) < (ROPE_DIM // 2)
    angle = jnp.where(in_a, grid_row, grid_col).astype(F32) * inverse
    is_u = (lane % (2 * quarter)) < quarter
    cosine = jnp.cos(angle)
    sine = jnp.where(is_u, -jnp.sin(angle), jnp.sin(angle))

    def rotated(pre):
        wide = pre.astype(BF16).astype(F32)
        swapped = jnp.where(is_u, pltpu.roll(wide, 128 - quarter, 1), pltpu.roll(wide, quarter, 1))
        return wide * cosine + swapped * sine

    pl.semaphore_wait(barrier, n_sp + n_fs - 1)

    def remote(src, dst, sem, device):
        return pltpu.make_async_remote_copy(
            src_ref=src,
            dst_ref=dst,
            send_sem=send_sem.at[sem],
            recv_sem=recv_sem.at[sem],
            device_id=device,
            device_id_type=MESH,
        )

    mate = {"tp": 1 - t}
    l_tok.wait()
    c_tok = remote(tok.at[t], tok.at[t], 0, mate)
    c_tok.start()
    l_gain.wait()
    c_gain = remote(gain.at[t], gain.at[t], 1, mate)
    c_gain.start()

    chunks = 4
    chunk_rows = depth // chunks
    sends = [c_tok, c_gain]
    hops = n_fs == 4
    if hops:
        near = f + 1 - 2 * (f % 2)
        far = (f + 2) % 4
        through = near * (1 - t) + far * t
        onward = far * (1 - t) + near * t
        across = 3 - f
        partners = (near, far)
    else:
        partners = tuple((f + j) % n_fs for j in range(1, n_fs))
    senders = partners if hops else tuple((f + n_fs - j) % n_fs for j in range(1, n_fs))

    def spread_out(ref, base, first, size):
        for j, peer in enumerate(partners):
            copy = remote(
                down(ref, f, first, size), down(ref, f, first, size), base + j, {"fs": peer}
            )
            copy.start()
            sends.append(copy)

    def take(ref, owner, sem, first=0, size=depth):
        remote(
            down(ref, owner, first, size), down(ref, owner, first, size), sem, mate
        ).wait_recv()

    width = n_fs - 1
    b_kv = 8

    def b_q(chunk):
        return 8 + (1 + chunk) * width

    def spread_q(chunk):
        spread_out(wq_all, b_q(chunk), chunk * chunk_rows, chunk_rows)

    l_kv.wait()
    spread_out(wkv_all, b_kv, 0, depth)
    l_q.wait()
    spread_q(0)

    remote(gain.at[1 - t], gain.at[1 - t], 1, mate).wait_recv()
    remote(tok.at[1 - t], tok.at[1 - t], 0, mate).wait_recv()
    whole = jnp.concatenate([tok[0], tok[1]], axis=1).astype(F32)
    lines = gain.shape[1]
    wide_gain = [gain[0].astype(F32), gain[1].astype(F32)]
    flat_gain = jnp.concatenate(
        [side[i : i + 1, :] for side in wide_gain for i in range(lines)], axis=1
    )
    hid[...] = normed(whole, flat_gain)

    own_rows = pl.ds(pl.multiple_of(s * rows, rows), rows)

    def rows_of(owner):
        return pl.ds(pl.multiple_of(owner * rows, rows), rows)

    def over_sp(ref, pool_send, pool_recv, j, device):
        return pltpu.make_async_remote_copy(
            src_ref=ref,
            dst_ref=ref,
            send_sem=pool_send.at[j],
            recv_sem=pool_recv.at[j],
            device_id=device,
            device_id_type=MESH,
        )

    def rope_copy(j, owner, device):
        return over_sp(ropes.at[owner], rope_send, rope_recv, j - 1, device)

    def gathered(j, owner, device):
        return over_sp(kvp.at[t, rows_of(owner)], gather_send, gather_recv, j - 1, device)

    def passed(j, owner, which):
        return over_sp(kvp.at[which, rows_of(owner)], pass_send, pass_recv, j - 1, mate)

    def relay(ref, sem, first=0, size=depth):
        part = down(ref, through, first, size)
        copy = remote(part, part, sem, {"fs": onward})
        copy.start()
        sends.append(copy)

    def relay_q(chunk):
        if hops:
            for j in range(2):
                take(wq_all, senders[j], b_q(chunk) + j, chunk * chunk_rows, chunk_rows)
            relay(wq_all, b_q(chunk) + 2, chunk * chunk_rows, chunk_rows)

    if hops:
        for j in range(2):
            take(wkv_all, senders[j], b_kv + j)
        relay(wkv_all, b_kv + 2)

    l_pi.wait()
    pool_in = mm(hid[...], wpi[...]).astype(BF16)
    halo_out[0] = pool_in[rows - 2 * RIM :, :].astype(F32)[RIM:, :]
    halo_out[1] = pool_in[: 2 * RIM, :].astype(F32)[:RIM, :]
    c_up = remote(halo_out.at[0], halo_in.at[0], 2, {"sp": (s + 1) % n_sp})
    c_dn = remote(halo_out.at[1], halo_in.at[1], 3, {"sp": (s + n_sp - 1) % n_sp})
    has_prev, has_next = s > 0, s < n_sp - 1
    pl.when(has_next)(c_up.start)
    pl.when(has_prev)(c_dn.start)

    for chunk in range(1, chunks):
        spread_q(chunk)

    l_kr.wait()
    key_pre = mm_t(hid[...], wkr[...])
    key_rope = rotated(jnp.concatenate([key_pre, key_pre], axis=1))
    lower_half = lax.broadcasted_iota(jnp.int32, (half, 128), 1) < ROPE_DIM
    ropes[s] = jnp.where(lower_half, key_rope[:half], key_rope[half:]).astype(BF16)
    for j in range(1, n_sp):
        copy = rope_copy(j, s, {"sp": (s + j) % n_sp})
        copy.start()
        sends.append(copy)

    relay_q(0)
    def no_rim(side):
        def clear():
            halo_in[side] = jnp.zeros(halo_in.shape[1:], F32)

        return clear

    pl.when(has_prev)(c_up.wait_recv)
    pl.when(has_next)(c_dn.wait_recv)
    pl.when(s == 0)(no_rim(0))
    pl.when(s == n_sp - 1)(no_rim(1))
    halo = jnp.concatenate([halo_in[0], halo_in[1]], axis=0).astype(BF16)
    padded = jnp.concatenate([pool_in, halo], axis=0)
    span = rows + 2 * RIM
    k_index = lax.broadcasted_iota(jnp.int32, (rows, span), 1)
    q_index = lax.broadcasted_iota(jnp.int32, (rows, span), 0)
    k_place = jnp.where(
        k_index < rows,
        k_index,
        jnp.where(k_index < rows + RIM, k_index - rows - RIM, k_index - RIM),
    )
    offset = k_place - q_index
    inside = (k_place + s * rows >= 0) & (k_place + s * rows < length)
    l_mix.wait()
    pooled = []
    for g in range(groups):
        group = t * groups + g
        window = jnp.int32(0)
        for index, size in enumerate(WINDOWS):
            window = jnp.where(group == index, size, window)
        before = window // 2
        band = jnp.where(
            inside & (offset >= -before) & (offset < window - before), 1.0, 0.0
        )
        count = jnp.sum(band, axis=1, keepdims=True)
        cols = slice(g * POOL_GROUP, (g + 1) * POOL_GROUP)
        mean = (mm(band.astype(BF16), padded[:, cols]) / count).astype(BF16)
        spread = (mean.astype(F32) - pool_in[:, cols].astype(F32)).astype(BF16)
        pooled.append(mm(spread, mix[g]).astype(BF16))
    l_op.wait()
    acc[...] = mm(jnp.concatenate(pooled, axis=1), wop[...])

    if hops:
        take(wkv_all, across, b_kv + 2)
    else:
        for j, owner in enumerate(senders):
            take(wkv_all, owner, b_kv + j)
    kvp[t, own_rows] = mm(hid[...], wkv_all[...]).astype(BF16)
    for j in range(1, n_sp):
        copy = gathered(j, s, {"sp": (s + j) % n_sp})
        copy.start()
        sends.append(copy)
    c_kvp = remote(kvp.at[t, rows_of(s)], kvp.at[t, rows_of(s)], 4, mate)
    c_kvp.start()
    sends.append(c_kvp)

    relay_q(1)
    relay_q(2)
    relay_q(3)
    shards = (f,) + senders
    last = shards[:1]
    if hops:
        last = (across,)
    else:
        for chunk in range(chunks):
            for j, owner in enumerate(senders):
                take(wq_all, owner, b_q(chunk) + j, chunk * chunk_rows, chunk_rows)
        shards = senders

    def from_shard(owner):
        start = pl.multiple_of(owner * depth, depth)
        return mm(hid[:, pl.ds(start, depth)], wq_all[pl.ds(start, depth), :])

    q_sum = functools.reduce(jnp.add, [from_shard(owner) for owner in shards])
    for j in range(1, n_sp):
        owner = (s + n_sp - j) % n_sp
        gathered(j, owner, mate).wait_recv()
        copy = passed(j, owner, t)
        copy.start()
        sends.append(copy)

    l_kvg.wait()

    def finish_keys(owner):
        here = rows_of(owner)
        kv_pre = jnp.concatenate([kvp[0, here], kvp[1, here]], axis=1).astype(F32)
        kcat[here, :kv_rank] = normed(kv_pre, kvg[...])
        packed = ropes[owner].astype(F32)
        swapped = pltpu.roll(packed, ROPE_DIM, 1)
        low = jnp.where(lower_half, packed, swapped)
        high = jnp.where(lower_half, swapped, packed)
        kcat[here, kv_rank:] = jnp.concatenate([low, high], axis=0).astype(BF16)

    remote(kvp.at[1 - t, rows_of(s)], kvp.at[1 - t, rows_of(s)], 4, mate).wait_recv()
    finish_keys(s)
    for j in range(1, n_sp):
        owner = (s + n_sp - j) % n_sp
        rope_copy(j, owner, mate).wait_recv()
        passed(j, owner, 1 - t).wait_recv()
        finish_keys(owner)

    if hops:
        for chunk in range(chunks):
            take(wq_all, across, b_q(chunk) + 2, chunk * chunk_rows, chunk_rows)
    q_sum = functools.reduce(jnp.add, [from_shard(owner) for owner in last], q_sum)
    qp[t] = q_sum.astype(BF16)
    c_qp = remote(qp.at[t], qp.at[t], 5, mate)
    c_qp.start()
    sends.append(c_qp)

    l_qg.wait()
    remote(qp.at[1 - t], qp.at[1 - t], 5, mate).wait_recv()
    q_latent = normed(jnp.concatenate([qp[0], qp[1]], axis=1).astype(F32), qg[...])
    l_qn.wait()
    q_nope = mm(q_latent, wqn[...]).astype(BF16)
    l_qr.wait()
    q_pre = mm(q_latent, wqr[...])
    l_ku.wait()
    low_lanes = lane < ROPE_DIM
    for h in range(heads):
        cols = slice(h * NOPE_DIM, (h + 1) * NOPE_DIM)
        absorbed = mm_t(q_nope[:, cols], wku[:, cols]).astype(BF16)
        if h % 2 == 0:
            turned = rotated(q_pre[:, h * ROPE_DIM : (h + 2) * ROPE_DIM])
        rope = jnp.where(low_lanes if h % 2 == 0 else ~low_lanes, turned, 0.0).astype(BF16)
        for part in range(2):
            piece = slice(part * half, (part + 1) * half)
            qcat[part, h * half : (h + 1) * half, :kv_rank] = absorbed[piece]
            qcat[part, h * half : (h + 1) * half, kv_rank:] = rope[piece]

    factor = (NOPE_DIM + ROPE_DIM) ** (-0.5) * math.log2(math.e)
    span_keys = rows * max(
        c for c in range(1, n_sp + 1) if n_sp % c == 0 and (c == 1 or rows * c <= SPAN_LIMIT)
    )
    spans = length // span_keys
    block = 4 * half

    def attend(part):
        def one_block(b, carry):
            block_rows = pl.ds(pl.multiple_of(b * block, block), block)
            queries = qcat[part, block_rows, :]

            def absorb(keys, state):
                scores = mm_t(queries, keys)
                top = jnp.max(scores, axis=1, keepdims=True)
                if state is not None:
                    top = jnp.maximum(top, state[0])
                weights = jnp.exp2((scores - top) * factor)
                total = jnp.sum(weights, axis=1, keepdims=True)
                summed = mm(weights.astype(BF16), keys[:, :kv_rank])
                if state is not None:
                    shrink = jnp.exp2((state[0] - top) * factor)
                    total = total + state[1] * shrink
                    summed = summed + state[2] * shrink
                return top, total, summed

            if spans == 1:
                state = absorb(kcat[...], None)
            else:
                state = absorb(kcat[:span_keys, :], None)

                def step(i, now):
                    start = pl.multiple_of(i * span_keys, span_keys)
                    return absorb(kcat[pl.ds(start, span_keys), :], now)

                state = lax.fori_loop(1, spans, step, state)
            ctx[block_rows, :] = (state[2] / state[1]).astype(BF16)
            return carry

        lax.fori_loop(0, heads * half // block, one_block, 0, unroll=True)
        for h in range(heads):
            cols = slice(h * VALUE_DIM, (h + 1) * VALUE_DIM)
            att[:, cols] = mm(ctx[h * half : (h + 1) * half, :], wvu[:, cols]).astype(BF16)
        own = acc[pl.ds(pl.multiple_of(part * half, half), half), :]
        return own + mm(att[...], woa[...])

    l_vu.wait()
    l_oa.wait()
    share[...] = attend(1 - t).astype(BF16)
    c_share = remote(share, arrived, 6, mate)
    c_share.start()
    sends.append(c_share)
    mine = attend(t)
    c_share.wait_recv()
    out[0] = (mine + arrived[...].astype(F32)).astype(BF16)
    pl.when(has_next)(c_up.wait_send)
    pl.when(has_prev)(c_dn.wait_send)
    for copy in sends:
        copy.wait_send()


def solution(mesh):
    n_sp, n_fs = mesh.shape["sp"], mesh.shape["fs"]

    def on_device(*args):
        args = list(args)
        args[1] = args[1].reshape(-1, 128)
        for i in (3, 7):
            args[i] = args[i].reshape(1, -1)
        args[10] = args[10].T
        (tokens, gain, wqd, qg, wqn, wqr, wkvd, kvg, wku, wvu, wkr, wpi, mix, woa, wop) = args
        rows, cols = tokens.shape[1:]
        half = rows // 2
        heads = wqn.shape[1] // NOPE_DIM
        kv_rank = wkvd.shape[1]
        q_rank = wqd.shape[1]
        d_model = woa.shape[1]
        groups = wpi.shape[1] // POOL_GROUP
        n_sems = 8 + 5 * (n_fs - 1)

        def vmem(*shape, kind=BF16):
            return pltpu.VMEM(shape, kind)

        def same(array):
            return pltpu.VMEM(array.shape, array.dtype)

        dma = pltpu.SemaphoreType.DMA
        return pl.pallas_call(
            functools.partial(layer, n_sp, n_fs),
            out_shape=jax.ShapeDtypeStruct((1, half, d_model), BF16),
            in_specs=[pl.BlockSpec(memory_space=pl.ANY)] * len(args),
            out_specs=pl.BlockSpec(memory_space=pltpu.VMEM),
            scratch_shapes=[
                vmem(2, rows, cols),
                vmem(2, cols // 128, 128),
                vmem(rows, 2 * cols),
                vmem(n_fs * wqd.shape[0], q_rank // 2),
                vmem(n_fs * wkvd.shape[0], kv_rank // 2),
                same(qg),
                same(kvg),
                same(wqn),
                same(wqr),
                same(wku),
                same(wvu),
                same(wkr),
                same(wpi),
                vmem(groups, POOL_GROUP, POOL_GROUP),
                same(woa),
                same(wop),
                vmem(2, RIM, wpi.shape[1], kind=F32),
                vmem(2, RIM, wpi.shape[1], kind=F32),
                vmem(2, n_sp * rows, kv_rank // 2),
                vmem(2, rows, q_rank // 2),
                vmem(n_sp, half, 2 * ROPE_DIM),
                vmem(n_sp * rows, kv_rank + 2 * ROPE_DIM),
                vmem(2, heads * half, kv_rank + 2 * ROPE_DIM),
                vmem(heads * half, kv_rank),
                vmem(half, heads * VALUE_DIM),
                vmem(rows, d_model, kind=F32),
                vmem(half, d_model),
                vmem(half, d_model),
                dma((16,)),
                dma((n_sems,)),
                dma((n_sems,)),
                dma((n_sp - 1,)),
                dma((n_sp - 1,)),
                dma((n_sp - 1,)),
                dma((n_sp - 1,)),
                dma((n_sp - 1,)),
                dma((n_sp - 1,)),
            ],
            compiler_params=pltpu.CompilerParams(collective_id=0, has_side_effects=True),
        )(*args)

    placed = (
        P("fs", "sp", "tp"),
        P("tp"),
        P("fs", None),
        P(),
        P(None, "tp"),
        P(None, "tp"),
        P("fs", None),
        P(),
        P(None, "tp"),
        P(None, "tp"),
        P(),
        P(None, "tp"),
        P(),
        P("tp", None),
        P("tp", None),
    )
    return jax.shard_map(
        on_device,
        mesh=mesh,
        in_specs=placed,
        out_specs=P("fs", ("sp", "tp"), None),
        check_vma=False,
    )
```

profile of v0, /device:TPU:0, one launch (start us, length us, event | category | flops | bytes accessed | tf_op | source)
XLA Modules:
  0.0 31.7 jit_solution(1488636652989235149)
XLA Ops:
  0.0 29.9 %shard_map.145 = bf16[1,96,2048]{2,1,0:T(8,128)(2,1)} custom-call(bf16[1,192,1024]{2,1,0:T(8,128)(2,1)} %tokens.1, bf16[8,128]{1,0:T(8,128)(2,1)} %bitcast.5, bf16[512,512]{1,0:T(8,128)(2,1)} %w_q_down.1, f32[1,512]{1,0:T(1,128)} %bitcast.6, bf16[512,1024]{1,0:T(8,128)(2,1)} %w_q_nope.1, bf16[512,512]{1,0:T(8,128)(2,1)} %w_q_rope.1, ...), custom_call_target="tpu_custom_call" | custom-call | tf_op jit(solution)/shard_map/pallas_call | solution.py:542
  29.9 1.8 %copy.17 = bf16[1,96,2048]{2,1,0:T(8,128)(2,1)} copy(bf16[1,96,2048]{2,1,0:T(8,128)(2,1)} %shard_map.145) | data formatting | bytes 786432
where the time goes:
time: 32 us; the launch traced here: 31.7 us
  Pallas kernels  29.9 us (93%)
  local copies, waits for them, and re-layouts  1.77 us (6%)
    pallas_call x1, Pallas kernels, on_device(): pl.pallas_call(functools.partial(layer, n_sp, n_fs), out_shape=jax.ShapeD...  29.9 us
    unnamed x1, local copies, waits for them, and re-layouts  1.77 us

commit v1 on v0

--- a/solution.py
+++ b/solution.py
@@ -541,8 +541,8 @@
         dma = pltpu.SemaphoreType.DMA
         return pl.pallas_call(
             functools.partial(layer, n_sp, n_fs),
-            out_shape=jax.ShapeDtypeStruct((1, half, d_model), BF16),
-            in_specs=[pl.BlockSpec(memory_space=pl.ANY)] * len(args),
+            out_shape=pltpu.VMEM((1, half, d_model), BF16),
+            in_specs=[pl.BlockSpec(memory_space=pltpu.HBM)] * len(args),
             out_specs=pl.BlockSpec(memory_space=pltpu.VMEM),
             scratch_shapes=[
                 vmem(2, rows, cols),
@@ -583,8 +583,8 @@
                 dma((n_sp - 1,)),
                 dma((n_sp - 1,)),
             ],
-            compiler_params=pltpu.CompilerParams(collective_id=0, has_side_effects=True),
-        )(*args)
+            compiler_params=pltpu.CompilerParams(collective_id=0, has_side_effects=True, vmem_limit_bytes=40 * 1024 * 1024),
+        )(*[pltpu.with_memory_space_constraint(a, pltpu.HBM) for a in args])
 
     placed = (
         P("fs", "sp", "tp"),

time: 32 us -> 30.3 us (0.947)
  local copies, waits for them, and re-layouts: 1.77 us -> 0.75 us
  Pallas kernels: 29.9 us -> 29.1 us
    unnamed x1, local copies, waits for them, and re-layouts: 1.77 us -> 0.75 us
    pallas_call x1, Pallas kernels: 29.9 us -> 29.1 us  [on_device(): pl.pallas_call(functools.partial(layer, n_sp, n_fs), out_shape=pltpu.VMEM...]
where the time goes in v1:
time: 30.3 us; the launch traced here: 29.9 us
  Pallas kernels  29.1 us (96%)
  local copies, waits for them, and re-layouts  0.75 us (2%)
    pallas_call x1, Pallas kernels, on_device(): pl.pallas_call(functools.partial(layer, n_sp, n_fs), out_shape=pltpu.VMEM...  29.1 us
    unnamed x1, local copies, waits for them, and re-layouts  0.75 us

profile of v1, /device:TPU:0, one launch (start us, length us, event | category | flops | bytes accessed | tf_op | source)
XLA Modules:
  0.0 29.9 jit_solution(2038128386259865089)
XLA Ops:
  0.0 29.1 %shard_map.145 = bf16[1,96,2048]{2,1,0:T(8,128)(2,1)S(1)} custom-call(bf16[1,192,1024]{2,1,0:T(8,128)(2,1)} %tokens.1, bf16[8,128]{1,0:T(8,128)(2,1)} %bitcast.5, bf16[512,512]{1,0:T(8,128)(2,1)} %w_q_down.1, f32[1,512]{1,0:T(1,128)} %bitcast.6, bf16[512,1024]{1,0:T(8,128)(2,1)} %w_q_nope.1, bf16[512,512]{1,0:T(8,128)(2,1)} %w_q_rope.1, ...), custom_call_target="tpu_custom_call" | custom-call | tf_op jit(solution)/shard_map/pallas_call | solution.py:542
  29.2 0.7 %copy.17 = bf16[1,96,2048]{2,1,0:T(8,128)(2,1)} copy(bf16[1,96,2048]{2,1,0:T(8,128)(2,1)S(1)} %shard_map.145) | data formatting | bytes 786432

commit v2 on v1

--- a/solution.py
+++ b/solution.py
@@ -21,6 +21,7 @@
 F32 = jnp.float32
 BF16 = jnp.bfloat16
 MESH = pl.DeviceIdType.MESH
+USE_Z = False
 
 
 def mm(a, b):
@@ -73,8 +74,9 @@
     wop,
     halo_out,
     halo_in,
-    kvp,
-    qp,
+    q_part,
+    q_lat,
+    kv_lat,
     ropes,
     kcat,
     qcat,
@@ -92,6 +94,7 @@
     pass_recv,
     rope_send,
     rope_recv,
+    word,
 ):
     s = lax.axis_index("sp")
     f = lax.axis_index("fs")
@@ -99,25 +102,21 @@
     rows = tok.shape[1]
     half = rows // 2
     depth = w_q_down.shape[0]
-    q_half = wq_all.shape[1]
-    kv_half = wkv_all.shape[1]
-    kv_rank = 2 * kv_half
+    kv_rank = wkv_all.shape[1]
+    kv_core, q_core = t == 1, t == 0
     heads = wqn.shape[1] // NOPE_DIM
     groups = wpi.shape[1] // POOL_GROUP
     length = rows * n_sp
 
-    def col(ref, width):
-        return ref.at[:, pl.ds(pl.multiple_of(t * width, width), width)]
-
     def down(ref, owner, first=0, size=depth):
         start = pl.multiple_of(owner * depth + first, 16)
         return ref.at[pl.ds(start, size), :]
 
     pairs = (
+        (w_kv_down, down(wkv_all, f)),
         (tokens.at[0], tok.at[t]),
         (norm_gain, gain.at[t]),
-        (col(w_kv_down, kv_half), down(wkv_all, f)),
-        (col(w_q_down, q_half), down(wq_all, f)),
+        (w_q_down, down(wq_all, f)),
         (w_k_rope, wkr),
         (w_pool_in, wpi),
         (kv_gain, kvg),
@@ -133,12 +132,10 @@
     loads = [
         pltpu.make_async_copy(src, dst, local_sem.at[i]) for i, (src, dst) in enumerate(pairs)
     ]
-    for load in loads:
-        load.start()
     (
+        l_kv,
         l_tok,
         l_gain,
-        l_kv,
         l_q,
         l_kr,
         l_pi,
@@ -152,22 +149,170 @@
         l_vu,
         l_oa,
     ) = loads
-
-    def signal_all():
-        barrier = pltpu.get_barrier_semaphore()
-        pl.semaphore_signal(barrier, inc=1, device_id={"tp": 1 - t}, device_id_type=MESH)
+    for load in loads:
+        if load is l_kv:
+            pl.when(kv_core)(load.start)
+        elif load is l_q:
+            pl.when(q_core)(load.start)
+        else:
+            load.start()
+
+    barrier = pltpu.get_barrier_semaphore()
+
+    def greet(device):
+        pl.semaphore_signal(barrier, inc=1, device_id=device, device_id_type=MESH)
+
+    hops = n_fs == 4
+    line = hops and n_sp == 4
+    has_prev, has_next = s > 0, s < n_sp - 1
+    mate = {"tp": 1 - t}
+    above, below = {"sp": (s + 1) % n_sp}, {"sp": (s + n_sp - 1) % n_sp}
+    parity = s % 2
+    if hops:
+        near = f + 1 - 2 * (f % 2)
+        far = (f + 2) % 4
+        across = 3 - f
+    greet(mate)
+    if line:
+        greet({"fs": near})
+        greet({"fs": far})
+        pl.when(has_next)(lambda: greet(above))
+        pl.when(has_prev)(lambda: greet(below))
+        guests = 5 - (s == 0).astype(jnp.int32) - (s == n_sp - 1).astype(jnp.int32)
+    else:
         for j in range(1, n_fs):
-            pl.semaphore_signal(
-                barrier, inc=1, device_id={"fs": (f + j) % n_fs}, device_id_type=MESH
-            )
+            greet({"fs": (f + j) % n_fs})
         for j in range(1, n_sp):
-            pl.semaphore_signal(
-                barrier, inc=1, device_id={"sp": (s + j) % n_sp}, device_id_type=MESH
-            )
-        return barrier
-
-    barrier = signal_all()
-
+            greet({"sp": (s + j) % n_sp})
+        guests = n_sp + n_fs - 1
+    pl.semaphore_wait(barrier, guests)
+
+    def tell(side, device):
+        pl.semaphore_signal(word.at[side], inc=1, device_id=device, device_id_type=MESH)
+
+    def hear(side, count):
+        return lambda: pl.semaphore_wait(word.at[side], count)
+
+    if line:
+
+        def both_ways():
+            tell(0, above)
+            tell(1, below)
+
+        pl.when(has_prev & has_next)(both_ways)
+
+    def spread_word():
+        def up():
+            hear(0, 1)()
+            tell(0, above)
+
+        def down_():
+            hear(1, 1)()
+            tell(1, below)
+
+        pl.when(s == n_sp - 2)(up)
+        pl.when(s == 1)(down_)
+
+    def hear_word():
+        pl.when(s == n_sp - 1)(hear(0, 2))
+        pl.when(s == 0)(hear(1, 2))
+
+    def remote(src, dst, sem, device):
+        return pltpu.make_async_remote_copy(
+            src_ref=src,
+            dst_ref=dst,
+            send_sem=send_sem.at[sem],
+            recv_sem=recv_sem.at[sem],
+            device_id=device,
+            device_id_type=MESH,
+        )
+
+    chunks = 4
+    chunk_rows = depth // chunks
+    sends, kv_sends, q_sends = [], [], []
+    over_z = hops and n_sp % 2 == 0 and USE_Z
+    if hops:
+        partners = senders = (near, far)
+    else:
+        partners = tuple((f + j) % n_fs for j in range(1, n_fs))
+        senders = tuple((f + n_fs - j) % n_fs for j in range(1, n_fs))
+    width = max(n_fs - 1, 4)
+    b_kv = 8
+    b_z = 8 + (1 + chunks) * width
+
+    def b_q(turn):
+        return 8 + (1 + turn) * width
+
+    def piece_at(turn):
+        if over_z:
+            return ((3 - parity), 0, 1, (2 + parity))[turn] * chunk_rows
+        return turn * chunk_rows
+
+    turns = range(chunks - 1) if over_z else range(chunks)
+
+    def outgoing(ref, base, first, size):
+        part = down(ref, f, first, size)
+        return [remote(part, part, base + j, {"fs": peer}) for j, peer in enumerate(partners)]
+
+    def incoming(ref, base, first, size):
+        return [
+            remote(part, part, base + j, mate)
+            for j, part in enumerate(down(ref, owner, first, size) for owner in senders)
+        ]
+
+    def onward(ref, base, first, size):
+        piece = size // 2
+        low, high = down(ref, near, first, piece), down(ref, far, first + piece, piece)
+        return [remote(low, low, base + 2, {"fs": far}), remote(high, high, base + 3, {"fs": near})]
+
+    def across_in(ref, base, first, size):
+        piece = size // 2
+        parts = (down(ref, across, first, piece), down(ref, across, first + piece, piece))
+        return [remote(part, part, base + 2 + j, mate) for j, part in enumerate(parts)]
+
+    def start(copies, pool):
+        for copy in copies:
+            copy.start()
+        pool += copies
+
+    def arrive(copies):
+        for copy in copies:
+            copy.wait_recv()
+
+    kv_out = outgoing(wkv_all, b_kv, 0, depth)
+    kv_in = incoming(wkv_all, b_kv, 0, depth)
+    q_out = [outgoing(wq_all, b_q(turn), piece_at(turn), chunk_rows) for turn in turns]
+    q_in = [incoming(wq_all, b_q(turn), piece_at(turn), chunk_rows) for turn in turns]
+    if hops:
+        kv_on = onward(wkv_all, b_kv, 0, depth)
+        kv_across = across_in(wkv_all, b_kv, 0, depth)
+        q_on = [onward(wq_all, b_q(turn), piece_at(turn), chunk_rows) for turn in turns]
+        q_across = [across_in(wq_all, b_q(turn), piece_at(turn), chunk_rows) for turn in turns]
+    else:
+        kv_on, kv_across = [], []
+        q_on = q_across = [[] for turn in turns]
+    if over_z:
+        over = {"sp": s + 1 - 2 * parity}
+        z_owners = (near, far, across)
+
+        def z_pieces(turn):
+            parts = [down(wq_all, owner, piece_at(turn), chunk_rows) for owner in z_owners]
+            return [remote(part, part, b_z + j, over) for j, part in enumerate(parts)]
+
+        z_out, z_in = z_pieces(0), z_pieces(chunks - 1)
+
+    @pl.when(kv_core)
+    def _():
+        l_kv.wait()
+        start(kv_out, kv_sends)
+
+    l_tok.wait()
+    c_tok = remote(tok.at[t], tok.at[t], 0, mate)
+    c_tok.start()
+    l_gain.wait()
+    c_gain = remote(gain.at[t], gain.at[t], 1, mate)
+    c_gain.start()
+    sends += [c_tok, c_gain]
     lane = lax.broadcasted_iota(jnp.int32, (rows, 128), 1)
     place = s * rows + lax.broadcasted_iota(jnp.int32, (rows, 128), 0)
     quarter = ROPE_DIM // 4
@@ -186,68 +331,8 @@
         swapped = jnp.where(is_u, pltpu.roll(wide, 128 - quarter, 1), pltpu.roll(wide, quarter, 1))
         return wide * cosine + swapped * sine
 
-    pl.semaphore_wait(barrier, n_sp + n_fs - 1)
-
-    def remote(src, dst, sem, device):
-        return pltpu.make_async_remote_copy(
-            src_ref=src,
-            dst_ref=dst,
-            send_sem=send_sem.at[sem],
-            recv_sem=recv_sem.at[sem],
-            device_id=device,
-            device_id_type=MESH,
-        )
-
-    mate = {"tp": 1 - t}
-    l_tok.wait()
-    c_tok = remote(tok.at[t], tok.at[t], 0, mate)
-    c_tok.start()
-    l_gain.wait()
-    c_gain = remote(gain.at[t], gain.at[t], 1, mate)
-    c_gain.start()
-
-    chunks = 4
-    chunk_rows = depth // chunks
-    sends = [c_tok, c_gain]
-    hops = n_fs == 4
-    if hops:
-        near = f + 1 - 2 * (f % 2)
-        far = (f + 2) % 4
-        through = near * (1 - t) + far * t
-        onward = far * (1 - t) + near * t
-        across = 3 - f
-        partners = (near, far)
-    else:
-        partners = tuple((f + j) % n_fs for j in range(1, n_fs))
-    senders = partners if hops else tuple((f + n_fs - j) % n_fs for j in range(1, n_fs))
-
-    def spread_out(ref, base, first, size):
-        for j, peer in enumerate(partners):
-            copy = remote(
-                down(ref, f, first, size), down(ref, f, first, size), base + j, {"fs": peer}
-            )
-            copy.start()
-            sends.append(copy)
-
-    def take(ref, owner, sem, first=0, size=depth):
-        remote(
-            down(ref, owner, first, size), down(ref, owner, first, size), sem, mate
-        ).wait_recv()
-
-    width = n_fs - 1
-    b_kv = 8
-
-    def b_q(chunk):
-        return 8 + (1 + chunk) * width
-
-    def spread_q(chunk):
-        spread_out(wq_all, b_q(chunk), chunk * chunk_rows, chunk_rows)
-
-    l_kv.wait()
-    spread_out(wkv_all, b_kv, 0, depth)
-    l_q.wait()
-    spread_q(0)
-
+    if line:
+        spread_word()
     remote(gain.at[1 - t], gain.at[1 - t], 1, mate).wait_recv()
     remote(tok.at[1 - t], tok.at[1 - t], 0, mate).wait_recv()
     whole = jnp.concatenate([tok[0], tok[1]], axis=1).astype(F32)
@@ -263,6 +348,13 @@
     def rows_of(owner):
         return pl.ds(pl.multiple_of(owner * rows, rows), rows)
 
+    if n_sp == 4:
+        peers_to = (s + 1 - 2 * parity, (s + 2) % 4, 3 - s)
+        peers_from = peers_to
+    else:
+        peers_to = tuple((s + j) % n_sp for j in range(1, n_sp))
+        peers_from = tuple((s + n_sp - j) % n_sp for j in range(1, n_sp))
+
     def over_sp(ref, pool_send, pool_recv, j, device):
         return pltpu.make_async_remote_copy(
             src_ref=ref,
@@ -274,55 +366,58 @@
         )
 
     def rope_copy(j, owner, device):
-        return over_sp(ropes.at[owner], rope_send, rope_recv, j - 1, device)
-
-    def gathered(j, owner, device):
-        return over_sp(kvp.at[t, rows_of(owner)], gather_send, gather_recv, j - 1, device)
-
-    def passed(j, owner, which):
-        return over_sp(kvp.at[which, rows_of(owner)], pass_send, pass_recv, j - 1, mate)
-
-    def relay(ref, sem, first=0, size=depth):
-        part = down(ref, through, first, size)
-        copy = remote(part, part, sem, {"fs": onward})
-        copy.start()
-        sends.append(copy)
-
-    def relay_q(chunk):
-        if hops:
-            for j in range(2):
-                take(wq_all, senders[j], b_q(chunk) + j, chunk * chunk_rows, chunk_rows)
-            relay(wq_all, b_q(chunk) + 2, chunk * chunk_rows, chunk_rows)
-
-    if hops:
-        for j in range(2):
-            take(wkv_all, senders[j], b_kv + j)
-        relay(wkv_all, b_kv + 2)
+        return over_sp(ropes.at[owner], rope_send, rope_recv, j, device)
+
+    def latent(owner):
+        return kv_lat.at[rows_of(owner)]
+
+    c_own = remote(latent(s), latent(s), 4, mate)
+    gather_out = [
+        over_sp(latent(s), gather_send, gather_recv, j, {"sp": peer})
+        for j, peer in enumerate(peers_to)
+    ]
+    gather_in = [
+        over_sp(latent(owner), gather_send, gather_recv, j, mate)
+        for j, owner in enumerate(peers_from)
+    ]
+    passed = [
+        over_sp(latent(owner), pass_send, pass_recv, j, mate)
+        for j, owner in enumerate(peers_from)
+    ]
 
     l_pi.wait()
     pool_in = mm(hid[...], wpi[...]).astype(BF16)
     halo_out[0] = pool_in[rows - 2 * RIM :, :].astype(F32)[RIM:, :]
     halo_out[1] = pool_in[: 2 * RIM, :].astype(F32)[:RIM, :]
-    c_up = remote(halo_out.at[0], halo_in.at[0], 2, {"sp": (s + 1) % n_sp})
-    c_dn = remote(halo_out.at[1], halo_in.at[1], 3, {"sp": (s + n_sp - 1) % n_sp})
-    has_prev, has_next = s > 0, s < n_sp - 1
+    c_up = remote(halo_out.at[0], halo_in.at[0], 2, above)
+    c_dn = remote(halo_out.at[1], halo_in.at[1], 3, below)
     pl.when(has_next)(c_up.start)
     pl.when(has_prev)(c_dn.start)
 
-    for chunk in range(1, chunks):
-        spread_q(chunk)
+    @pl.when(q_core)
+    def _():
+        l_q.wait()
+        for copies in q_out:
+            start(copies, q_sends)
+
 
     l_kr.wait()
     key_pre = mm_t(hid[...], wkr[...])
     key_rope = rotated(jnp.concatenate([key_pre, key_pre], axis=1))
     lower_half = lax.broadcasted_iota(jnp.int32, (half, 128), 1) < ROPE_DIM
     ropes[s] = jnp.where(lower_half, key_rope[:half], key_rope[half:]).astype(BF16)
-    for j in range(1, n_sp):
-        copy = rope_copy(j, s, {"sp": (s + j) % n_sp})
+    if line:
+        hear_word()
+    for j, peer in enumerate(peers_to):
+        copy = rope_copy(j, s, {"sp": peer})
         copy.start()
         sends.append(copy)
 
-    relay_q(0)
+    @pl.when(kv_core)
+    def _():
+        arrive(kv_in)
+        start(kv_on, kv_sends)
+
     def no_rim(side):
         def clear():
             halo_in[side] = jnp.zeros(halo_in.shape[1:], F32)
@@ -364,77 +459,70 @@
     l_op.wait()
     acc[...] = mm(jnp.concatenate(pooled, axis=1), wop[...])
 
-    if hops:
-        take(wkv_all, across, b_kv + 2)
-    else:
-        for j, owner in enumerate(senders):
-            take(wkv_all, owner, b_kv + j)
-    kvp[t, own_rows] = mm(hid[...], wkv_all[...]).astype(BF16)
-    for j in range(1, n_sp):
-        copy = gathered(j, s, {"sp": (s + j) % n_sp})
-        copy.start()
-        sends.append(copy)
-    c_kvp = remote(kvp.at[t, rows_of(s)], kvp.at[t, rows_of(s)], 4, mate)
-    c_kvp.start()
-    sends.append(c_kvp)
-
-    relay_q(1)
-    relay_q(2)
-    relay_q(3)
-    shards = (f,) + senders
-    last = shards[:1]
-    if hops:
-        last = (across,)
-    else:
-        for chunk in range(chunks):
-            for j, owner in enumerate(senders):
-                take(wq_all, owner, b_q(chunk) + j, chunk * chunk_rows, chunk_rows)
-        shards = senders
-
-    def from_shard(owner):
-        start = pl.multiple_of(owner * depth, depth)
-        return mm(hid[:, pl.ds(start, depth)], wq_all[pl.ds(start, depth), :])
-
-    q_sum = functools.reduce(jnp.add, [from_shard(owner) for owner in shards])
-    for j in range(1, n_sp):
-        owner = (s + n_sp - j) % n_sp
-        gathered(j, owner, mate).wait_recv()
-        copy = passed(j, owner, t)
-        copy.start()
-        sends.append(copy)
-
     l_kvg.wait()
-
-    def finish_keys(owner):
+    l_qg.wait()
+
+    @pl.when(kv_core)
+    def _():
+        arrive(kv_across)
+        pre = mm(hid[...], wkv_all[...]).astype(BF16).astype(F32)
+        kv_lat[own_rows] = normed(pre, kvg[...])
+        start(gather_out + [c_own], kv_sends)
+
+    @pl.when(q_core)
+    def _():
+        for turn in turns:
+            arrive(q_in[turn])
+            start(q_on[turn], q_sends)
+            if over_z and turn == 0:
+                start(z_out[:2], q_sends)
+            if over_z and turn == 1:
+                arrive(q_across[0])
+                start(z_out[2:], q_sends)
+
+    def finish_rope(owner):
         here = rows_of(owner)
-        kv_pre = jnp.concatenate([kvp[0, here], kvp[1, here]], axis=1).astype(F32)
-        kcat[here, :kv_rank] = normed(kv_pre, kvg[...])
         packed = ropes[owner].astype(F32)
         swapped = pltpu.roll(packed, ROPE_DIM, 1)
         low = jnp.where(lower_half, packed, swapped)
         high = jnp.where(lower_half, swapped, packed)
         kcat[here, kv_rank:] = jnp.concatenate([low, high], axis=0).astype(BF16)
 
-    remote(kvp.at[1 - t, rows_of(s)], kvp.at[1 - t, rows_of(s)], 4, mate).wait_recv()
-    finish_keys(s)
-    for j in range(1, n_sp):
-        owner = (s + n_sp - j) % n_sp
+    finish_rope(s)
+    for j, owner in enumerate(peers_from):
         rope_copy(j, owner, mate).wait_recv()
-        passed(j, owner, 1 - t).wait_recv()
-        finish_keys(owner)
-
-    if hops:
-        for chunk in range(chunks):
-            take(wq_all, across, b_q(chunk) + 2, chunk * chunk_rows, chunk_rows)
-    q_sum = functools.reduce(jnp.add, [from_shard(owner) for owner in last], q_sum)
-    qp[t] = q_sum.astype(BF16)
-    c_qp = remote(qp.at[t], qp.at[t], 5, mate)
-    c_qp.start()
-    sends.append(c_qp)
-
-    l_qg.wait()
-    remote(qp.at[1 - t], qp.at[1 - t], 5, mate).wait_recv()
-    q_latent = normed(jnp.concatenate([qp[0], qp[1]], axis=1).astype(F32), qg[...])
+        finish_rope(owner)
+
+    c_lat = remote(q_lat, q_lat, 5, mate)
+
+    def from_shard(owner):
+        first = pl.multiple_of(owner * depth, depth)
+        return mm(hid[:, pl.ds(first, depth)], wq_all[pl.ds(first, depth), :])
+
+    @pl.when(kv_core)
+    def _():
+        for j in range(n_sp - 1):
+            gather_in[j].wait_recv()
+            start([passed[j]], kv_sends)
+        c_lat.wait_recv()
+
+    @pl.when(q_core)
+    def _():
+        if over_z:
+            arrive(z_in[:2])
+        q_part[...] = functools.reduce(jnp.add, [from_shard(owner) for owner in (f,) + senders])
+        for turn in turns:
+            if not (over_z and turn == 0):
+                arrive(q_across[turn])
+        if over_z:
+            arrive(z_in[2:])
+        q_sum = q_part[...]
+        if hops:
+            q_sum = q_sum + from_shard(across)
+        q_lat[...] = normed(q_sum.astype(BF16).astype(F32), qg[...])
+        start([c_lat], q_sends)
+
+    q_latent = q_lat[...]
     l_qn.wait()
     q_nope = mm(q_latent, wqn[...]).astype(BF16)
     l_qr.wait()
@@ -500,6 +588,13 @@
 
     l_vu.wait()
     l_oa.wait()
+
+    @pl.when(q_core)
+    def _():
+        c_own.wait_recv()
+        arrive(passed)
+
+    kcat[:, :kv_rank] = kv_lat[...]
     share[...] = attend(1 - t).astype(BF16)
     c_share = remote(share, arrived, 6, mate)
     c_share.start()
@@ -511,6 +606,16 @@
     pl.when(has_prev)(c_dn.wait_send)
     for copy in sends:
         copy.wait_send()
+
+    @pl.when(kv_core)
+    def _():
+        for copy in kv_sends:
+            copy.wait_send()
+
+    @pl.when(q_core)
+    def _():
+        for copy in q_sends:
+            copy.wait_send()
 
 
 def solution(mesh):
@@ -530,7 +635,7 @@
         q_rank = wqd.shape[1]
         d_model = woa.shape[1]
         groups = wpi.shape[1] // POOL_GROUP
-        n_sems = 8 + 5 * (n_fs - 1)
+        n_sems = 8 + 5 * max(n_fs - 1, 4) + 3
 
         def vmem(*shape, kind=BF16):
             return pltpu.VMEM(shape, kind)
@@ -548,8 +653,8 @@
                 vmem(2, rows, cols),
                 vmem(2, cols // 128, 128),
                 vmem(rows, 2 * cols),
-                vmem(n_fs * wqd.shape[0], q_rank // 2),
-                vmem(n_fs * wkvd.shape[0], kv_rank // 2),
+                vmem(n_fs * wqd.shape[0], q_rank),
+                vmem(n_fs * wkvd.shape[0], kv_rank),
                 same(qg),
                 same(kvg),
                 same(wqn),
@@ -563,8 +668,9 @@
                 same(wop),
                 vmem(2, RIM, wpi.shape[1], kind=F32),
                 vmem(2, RIM, wpi.shape[1], kind=F32),
-                vmem(2, n_sp * rows, kv_rank // 2),
-                vmem(2, rows, q_rank // 2),
+                vmem(rows, q_rank, kind=F32),
+                vmem(rows, q_rank),
+                vmem(n_sp * rows, kv_rank),
                 vmem(n_sp, half, 2 * ROPE_DIM),
                 vmem(n_sp * rows, kv_rank + 2 * ROPE_DIM),
                 vmem(2, heads * half, kv_rank + 2 * ROPE_DIM),
@@ -582,6 +688,7 @@
                 dma((n_sp - 1,)),
                 dma((n_sp - 1,)),
                 dma((n_sp - 1,)),
+                pltpu.SemaphoreType.REGULAR((2,)),
             ],
             compiler_params=pltpu.CompilerParams(collective_id=0, has_side_effects=True, vmem_limit_bytes=40 * 1024 * 1024),
         )(*[pltpu.with_memory_space_constraint(a, pltpu.HBM) for a in args])

time: 30.3 us -> 28.4 us (0.937)
  Pallas kernels: 29.1 us -> 27.5 us
    pallas_call x1, Pallas kernels: 29.1 us -> 27.5 us  [on_device(): pl.pallas_call(functools.partial(layer, n_sp, n_fs), out_shape=pltpu.VMEM...]
where the time goes in v2:
time: 28.4 us; the launch traced here: 28.3 us
  Pallas kernels  27.5 us (97%)
  local copies, waits for them, and re-layouts  0.75 us (3%)
    pallas_call x1, Pallas kernels, on_device(): pl.pallas_call(functools.partial(layer, n_sp, n_fs), out_shape=pltpu.VMEM...  27.5 us
    unnamed x1, local copies, waits for them, and re-layouts  0.75 us

profile of v2, /device:TPU:0, one launch (start us, length us, event | category | flops | bytes accessed | tf_op | source)
XLA Modules:
  0.0 28.3 jit_solution(17059563986443958261)
XLA Ops:
  0.0 27.5 %shard_map.145 = bf16[1,96,2048]{2,1,0:T(8,128)(2,1)S(1)} custom-call(bf16[1,192,1024]{2,1,0:T(8,128)(2,1)} %tokens.1, bf16[8,128]{1,0:T(8,128)(2,1)} %bitcast.5, bf16[512,512]{1,0:T(8,128)(2,1)} %w_q_down.1, f32[1,512]{1,0:T(1,128)} %bitcast.6, bf16[512,1024]{1,0:T(8,128)(2,1)} %w_q_nope.1, bf16[512,512]{1,0:T(8,128)(2,1)} %w_q_rope.1, ...), custom_call_target="tpu_custom_call" | custom-call | tf_op jit(solution)/shard_map/pallas_call | solution.py:647
  27.5 0.7 %copy.17 = bf16[1,96,2048]{2,1,0:T(8,128)(2,1)} copy(bf16[1,96,2048]{2,1,0:T(8,128)(2,1)S(1)} %shard_map.145) | data formatting | bytes 786432

commit v3 on v2

--- a/solution.py
+++ b/solution.py
@@ -21,7 +21,8 @@
 F32 = jnp.float32
 BF16 = jnp.bfloat16
 MESH = pl.DeviceIdType.MESH
-USE_Z = False
+TOK, GAIN, UP, DOWN, LATENT, SHARE, ROPE, STAGE = range(8)
+MAIN, GATHER, PASS, BLOCK, SIDE_A, SIDE_B = range(6)
 
 
 def mm(a, b):
@@ -88,12 +89,6 @@
     local_sem,
     send_sem,
     recv_sem,
-    gather_send,
-    gather_recv,
-    pass_send,
-    pass_recv,
-    rope_send,
-    rope_recv,
     word,
 ):
     s = lax.axis_index("sp")
@@ -129,8 +124,10 @@
         (w_v_up, wvu),
         (w_out_attn, woa),
     )
+    slots = (0, 1, 2, 0, 3, 3, 4, 5, 6, 6, 7, 7, 7, 7, 8)
     loads = [
-        pltpu.make_async_copy(src, dst, local_sem.at[i]) for i, (src, dst) in enumerate(pairs)
+        pltpu.make_async_copy(src, dst, local_sem.at[slot])
+        for slot, (src, dst) in zip(slots, pairs)
     ]
     (
         l_kv,
@@ -217,102 +214,82 @@
         pl.when(s == n_sp - 1)(hear(0, 2))
         pl.when(s == 0)(hear(1, 2))
 
-    def remote(src, dst, sem, device):
+    def remote(src, dst, sent, slot, device):
         return pltpu.make_async_remote_copy(
             src_ref=src,
             dst_ref=dst,
-            send_sem=send_sem.at[sem],
-            recv_sem=recv_sem.at[sem],
+            send_sem=send_sem.at[sent],
+            recv_sem=recv_sem.at[slot],
             device_id=device,
             device_id_type=MESH,
         )
 
+    def part_of(ref, count):
+        return ref.at[pl.ds(0, count)]
+
+    def all_sent(ref, count, sent):
+        part = part_of(ref, count)
+        remote(part, part, sent, TOK, mate).wait_send()
+
+    def all_taken(ref, count, slot):
+        part = part_of(ref, count)
+        remote(part, part, MAIN, slot, mate).wait_recv()
+
+    def all_loaded(*refs):
+        slot = {id(ref): i for ref, i in zip((dst for _, dst in pairs), slots)}[id(refs[0])]
+        line_bytes = 2 * woa.shape[1]
+        total = sum(math.prod(ref.shape) * ref.dtype.itemsize for ref in refs)
+        part = part_of(woa, total // line_bytes)
+        pltpu.make_async_copy(part, part, local_sem.at[slot]).wait()
+
     chunks = 4
     chunk_rows = depth // chunks
-    sends, kv_sends, q_sends = [], [], []
-    over_z = hops and n_sp % 2 == 0 and USE_Z
     if hops:
         partners = senders = (near, far)
     else:
         partners = tuple((f + j) % n_fs for j in range(1, n_fs))
         senders = tuple((f + n_fs - j) % n_fs for j in range(1, n_fs))
-    width = max(n_fs - 1, 4)
-    b_kv = 8
-    b_z = 8 + (1 + chunks) * width
-
-    def b_q(turn):
-        return 8 + (1 + turn) * width
-
     def piece_at(turn):
-        if over_z:
-            return ((3 - parity), 0, 1, (2 + parity))[turn] * chunk_rows
         return turn * chunk_rows
 
-    turns = range(chunks - 1) if over_z else range(chunks)
-
-    def outgoing(ref, base, first, size):
+    turns = range(chunks)
+
+    def outgoing(ref, slot, first, size):
         part = down(ref, f, first, size)
-        return [remote(part, part, base + j, {"fs": peer}) for j, peer in enumerate(partners)]
-
-    def incoming(ref, base, first, size):
-        return [
-            remote(part, part, base + j, mate)
-            for j, part in enumerate(down(ref, owner, first, size) for owner in senders)
-        ]
-
-    def onward(ref, base, first, size):
+        return [remote(part, part, MAIN, slot, {"fs": peer}) for peer in partners]
+
+    def onward(ref, slot, first, size):
         piece = size // 2
         low, high = down(ref, near, first, piece), down(ref, far, first + piece, piece)
-        return [remote(low, low, base + 2, {"fs": far}), remote(high, high, base + 3, {"fs": near})]
-
-    def across_in(ref, base, first, size):
-        piece = size // 2
-        parts = (down(ref, across, first, piece), down(ref, across, first + piece, piece))
-        return [remote(part, part, base + 2 + j, mate) for j, part in enumerate(parts)]
-
-    def start(copies, pool):
+        return [
+            remote(low, low, MAIN, slot, {"fs": far}),
+            remote(high, high, MAIN, slot, {"fs": near}),
+        ]
+
+    def start(copies):
         for copy in copies:
             copy.start()
-        pool += copies
-
-    def arrive(copies):
-        for copy in copies:
-            copy.wait_recv()
-
-    kv_out = outgoing(wkv_all, b_kv, 0, depth)
-    kv_in = incoming(wkv_all, b_kv, 0, depth)
-    q_out = [outgoing(wq_all, b_q(turn), piece_at(turn), chunk_rows) for turn in turns]
-    q_in = [incoming(wq_all, b_q(turn), piece_at(turn), chunk_rows) for turn in turns]
+
+    kv_out = outgoing(wkv_all, STAGE, 0, depth)
+    q_out = [outgoing(wq_all, STAGE + turn, piece_at(turn), chunk_rows) for turn in turns]
     if hops:
-        kv_on = onward(wkv_all, b_kv, 0, depth)
-        kv_across = across_in(wkv_all, b_kv, 0, depth)
-        q_on = [onward(wq_all, b_q(turn), piece_at(turn), chunk_rows) for turn in turns]
-        q_across = [across_in(wq_all, b_q(turn), piece_at(turn), chunk_rows) for turn in turns]
+        kv_on = onward(wkv_all, STAGE + 1, 0, depth)
+        last = STAGE + chunks
+        q_on = [onward(wq_all, last, piece_at(turn), chunk_rows) for turn in turns]
     else:
-        kv_on, kv_across = [], []
-        q_on = q_across = [[] for turn in turns]
-    if over_z:
-        over = {"sp": s + 1 - 2 * parity}
-        z_owners = (near, far, across)
-
-        def z_pieces(turn):
-            parts = [down(wq_all, owner, piece_at(turn), chunk_rows) for owner in z_owners]
-            return [remote(part, part, b_z + j, over) for j, part in enumerate(parts)]
-
-        z_out, z_in = z_pieces(0), z_pieces(chunks - 1)
-
+        kv_on = []
+        q_on = [[] for turn in turns]
     @pl.when(kv_core)
     def _():
         l_kv.wait()
-        start(kv_out, kv_sends)
+        start(kv_out)
 
     l_tok.wait()
-    c_tok = remote(tok.at[t], tok.at[t], 0, mate)
+    l_gain.wait()
+    c_tok = remote(tok.at[t], tok.at[t], SIDE_A, TOK, mate)
     c_tok.start()
-    l_gain.wait()
-    c_gain = remote(gain.at[t], gain.at[t], 1, mate)
+    c_gain = remote(gain.at[t], gain.at[t], SIDE_B, GAIN, mate)
     c_gain.start()
-    sends += [c_tok, c_gain]
     lane = lax.broadcasted_iota(jnp.int32, (rows, 128), 1)
     place = s * rows + lax.broadcasted_iota(jnp.int32, (rows, 128), 0)
     quarter = ROPE_DIM // 4
@@ -333,8 +310,8 @@
 
     if line:
         spread_word()
-    remote(gain.at[1 - t], gain.at[1 - t], 1, mate).wait_recv()
-    remote(tok.at[1 - t], tok.at[1 - t], 0, mate).wait_recv()
+    c_gain.wait()
+    c_tok.wait()
     whole = jnp.concatenate([tok[0], tok[1]], axis=1).astype(F32)
     lines = gain.shape[1]
     wide_gain = [gain[0].astype(F32), gain[1].astype(F32)]
@@ -355,42 +332,26 @@
         peers_to = tuple((s + j) % n_sp for j in range(1, n_sp))
         peers_from = tuple((s + n_sp - j) % n_sp for j in range(1, n_sp))
 
-    def over_sp(ref, pool_send, pool_recv, j, device):
-        return pltpu.make_async_remote_copy(
-            src_ref=ref,
-            dst_ref=ref,
-            send_sem=pool_send.at[j],
-            recv_sem=pool_recv.at[j],
-            device_id=device,
-            device_id_type=MESH,
-        )
-
-    def rope_copy(j, owner, device):
-        return over_sp(ropes.at[owner], rope_send, rope_recv, j, device)
-
-    def latent(owner):
-        return kv_lat.at[rows_of(owner)]
-
-    c_own = remote(latent(s), latent(s), 4, mate)
-    gather_out = [
-        over_sp(latent(s), gather_send, gather_recv, j, {"sp": peer})
-        for j, peer in enumerate(peers_to)
-    ]
-    gather_in = [
-        over_sp(latent(owner), gather_send, gather_recv, j, mate)
-        for j, owner in enumerate(peers_from)
-    ]
-    passed = [
-        over_sp(latent(owner), pass_send, pass_recv, j, mate)
-        for j, owner in enumerate(peers_from)
-    ]
-
-    l_pi.wait()
+    def rope_copy(owner, device):
+        return remote(ropes.at[owner], ropes.at[owner], BLOCK, ROPE, device)
+
+    def latent(owner, sent, slot, device):
+        here = kv_lat.at[rows_of(owner)]
+        return remote(here, here, sent, slot, device)
+
+    base = STAGE + 2
+    taken = LATENT
+    c_own = latent(s, GATHER, taken, mate)
+    gather_out = [latent(s, GATHER, base + j, {"sp": peer}) for j, peer in enumerate(peers_to)]
+    gather_in = [latent(owner, GATHER, base + j, mate) for j, owner in enumerate(peers_from)]
+    passed = [latent(owner, PASS, taken, mate) for owner in peers_from]
+
+    all_loaded(wkr, wpi)
     pool_in = mm(hid[...], wpi[...]).astype(BF16)
     halo_out[0] = pool_in[rows - 2 * RIM :, :].astype(F32)[RIM:, :]
     halo_out[1] = pool_in[: 2 * RIM, :].astype(F32)[:RIM, :]
-    c_up = remote(halo_out.at[0], halo_in.at[0], 2, above)
-    c_dn = remote(halo_out.at[1], halo_in.at[1], 3, below)
+    c_up = remote(halo_out.at[0], halo_in.at[0], SIDE_A, UP, above)
+    c_dn = remote(halo_out.at[1], halo_in.at[1], SIDE_B, DOWN, below)
     pl.when(has_next)(c_up.start)
     pl.when(has_prev)(c_dn.start)
 
@@ -398,25 +359,23 @@
     def _():
         l_q.wait()
         for copies in q_out:
-            start(copies, q_sends)
-
-
-    l_kr.wait()
+            start(copies)
+
+
     key_pre = mm_t(hid[...], wkr[...])
     key_rope = rotated(jnp.concatenate([key_pre, key_pre], axis=1))
     lower_half = lax.broadcasted_iota(jnp.int32, (half, 128), 1) < ROPE_DIM
     ropes[s] = jnp.where(lower_half, key_rope[:half], key_rope[half:]).astype(BF16)
     if line:
         hear_word()
-    for j, peer in enumerate(peers_to):
-        copy = rope_copy(j, s, {"sp": peer})
+    for peer in peers_to:
+        copy = rope_copy(s, {"sp": peer})
         copy.start()
-        sends.append(copy)
 
     @pl.when(kv_core)
     def _():
-        arrive(kv_in)
-        start(kv_on, kv_sends)
+        all_taken(wkv_all, len(senders) * depth, STAGE)
+        start(kv_on)
 
     def no_rim(side):
         def clear():
@@ -439,8 +398,10 @@
         jnp.where(k_index < rows + RIM, k_index - rows - RIM, k_index - RIM),
     )
     offset = k_place - q_index
+    l_kvg.wait()
+    l_qg.wait()
+    all_loaded(mix, wop)
     inside = (k_place + s * rows >= 0) & (k_place + s * rows < length)
-    l_mix.wait()
     pooled = []
     for g in range(groups):
         group = t * groups + g
@@ -456,29 +417,22 @@
         mean = (mm(band.astype(BF16), padded[:, cols]) / count).astype(BF16)
         spread = (mean.astype(F32) - pool_in[:, cols].astype(F32)).astype(BF16)
         pooled.append(mm(spread, mix[g]).astype(BF16))
-    l_op.wait()
     acc[...] = mm(jnp.concatenate(pooled, axis=1), wop[...])
 
-    l_kvg.wait()
-    l_qg.wait()
 
     @pl.when(kv_core)
     def _():
-        arrive(kv_across)
+        if hops:
+            all_taken(wkv_all, depth, STAGE + 1)
         pre = mm(hid[...], wkv_all[...]).astype(BF16).astype(F32)
         kv_lat[own_rows] = normed(pre, kvg[...])
-        start(gather_out + [c_own], kv_sends)
+        start(gather_out + [c_own])
 
     @pl.when(q_core)
     def _():
         for turn in turns:
-            arrive(q_in[turn])
-            start(q_on[turn], q_sends)
-            if over_z and turn == 0:
-                start(z_out[:2], q_sends)
-            if over_z and turn == 1:
-                arrive(q_across[0])
-                start(z_out[2:], q_sends)
+            all_taken(wq_all, len(senders) * chunk_rows, STAGE + turn)
+            start(q_on[turn])
 
     def finish_rope(owner):
         here = rows_of(owner)
@@ -488,12 +442,12 @@
         high = jnp.where(lower_half, swapped, packed)
         kcat[here, kv_rank:] = jnp.concatenate([low, high], axis=0).astype(BF16)
 
-    finish_rope(s)
-    for j, owner in enumerate(peers_from):
-        rope_copy(j, owner, mate).wait_recv()
+    all_taken(ropes, n_sp - 1, ROPE)
+    all_sent(ropes, n_sp - 1, BLOCK)
+    for owner in (s,) + peers_from:
         finish_rope(owner)
 
-    c_lat = remote(q_lat, q_lat, 5, mate)
+    c_lat = remote(q_lat, q_lat, GATHER, LATENT, mate)
 
     def from_shard(owner):
         first = pl.multiple_of(owner * depth, depth)
@@ -503,31 +457,25 @@
     def _():
         for j in range(n_sp - 1):
             gather_in[j].wait_recv()
-            start([passed[j]], kv_sends)
+            passed[j].start()
         c_lat.wait_recv()
 
     @pl.when(q_core)
     def _():
-        if over_z:
-            arrive(z_in[:2])
         q_part[...] = functools.reduce(jnp.add, [from_shard(owner) for owner in (f,) + senders])
-        for turn in turns:
-            if not (over_z and turn == 0):
-                arrive(q_across[turn])
-        if over_z:
-            arrive(z_in[2:])
+        if hops:
+            all_taken(wq_all, depth, STAGE + chunks)
         q_sum = q_part[...]
         if hops:
             q_sum = q_sum + from_shard(across)
         q_lat[...] = normed(q_sum.astype(BF16).astype(F32), qg[...])
-        start([c_lat], q_sends)
+        c_lat.start()
 
     q_latent = q_lat[...]
-    l_qn.wait()
+    all_loaded(wqn, wqr, wku, wvu)
+    l_oa.wait()
     q_nope = mm(q_latent, wqn[...]).astype(BF16)
-    l_qr.wait()
     q_pre = mm(q_latent, wqr[...])
-    l_ku.wait()
     low_lanes = lane < ROPE_DIM
     for h in range(heads):
         cols = slice(h * NOPE_DIM, (h + 1) * NOPE_DIM)
@@ -586,36 +534,31 @@
         own = acc[pl.ds(pl.multiple_of(part * half, half), half), :]
         return own + mm(att[...], woa[...])
 
-    l_vu.wait()
-    l_oa.wait()
 
     @pl.when(q_core)
     def _():
-        c_own.wait_recv()
-        arrive(passed)
+        all_taken(kv_lat, n_sp * rows, LATENT)
 
     kcat[:, :kv_rank] = kv_lat[...]
     share[...] = attend(1 - t).astype(BF16)
-    c_share = remote(share, arrived, 6, mate)
+    c_share = remote(share, arrived, BLOCK, SHARE, mate)
     c_share.start()
-    sends.append(c_share)
     mine = attend(t)
-    c_share.wait_recv()
+    c_share.wait()
     out[0] = (mine + arrived[...].astype(F32)).astype(BF16)
     pl.when(has_next)(c_up.wait_send)
     pl.when(has_prev)(c_dn.wait_send)
-    for copy in sends:
-        copy.wait_send()
 
     @pl.when(kv_core)
     def _():
-        for copy in kv_sends:
-            copy.wait_send()
+        all_sent(wkv_all, (n_fs - 1) * depth, MAIN)
+        all_sent(kv_lat, n_sp * rows, GATHER)
+        all_sent(kv_lat, (n_sp - 1) * rows, PASS)
 
     @pl.when(q_core)
     def _():
-        for copy in q_sends:
-            copy.wait_send()
+        all_sent(wq_all, (n_fs - 1) * depth, MAIN)
+        c_lat.wait_send()
 
 
 def solution(mesh):
@@ -635,7 +578,6 @@
         q_rank = wqd.shape[1]
         d_model = woa.shape[1]
         groups = wpi.shape[1] // POOL_GROUP
-        n_sems = 8 + 5 * max(n_fs - 1, 4) + 3
 
         def vmem(*shape, kind=BF16):
             return pltpu.VMEM(shape, kind)
@@ -679,15 +621,9 @@
                 vmem(rows, d_model, kind=F32),
                 vmem(half, d_model),
                 vmem(half, d_model),
-                dma((16,)),
-                dma((n_sems,)),
-                dma((n_sems,)),
-                dma((n_sp - 1,)),
-                dma((n_sp - 1,)),
-                dma((n_sp - 1,)),
-                dma((n_sp - 1,)),
-                dma((n_sp - 1,)),
-                dma((n_sp - 1,)),
+                dma((9,)),
+                dma((6,)),
+                dma((STAGE + max(5, n_sp + 1),)),
                 pltpu.SemaphoreType.REGULAR((2,)),
             ],
             compiler_params=pltpu.CompilerParams(collective_id=0, has_side_effects=True, vmem_limit_bytes=40 * 1024 * 1024),

time: 28.4 us -> 27.8 us (0.979)
  Pallas kernels: 27.5 us -> 26.9 us
    pallas_call x1, Pallas kernels: 27.5 us -> 26.9 us  [on_device(): pl.pallas_call(functools.partial(layer, n_sp, n_fs), out_shape=pltpu.VMEM...]
where the time goes in v3:
time: 27.8 us; the launch traced here: 27.6 us
  Pallas kernels  26.9 us (97%)
  local copies, waits for them, and re-layouts  0.75 us (3%)
    pallas_call x1, Pallas kernels, on_device(): pl.pallas_call(functools.partial(layer, n_sp, n_fs), out_shape=pltpu.VMEM...  26.9 us
    unnamed x1, local copies, waits for them, and re-layouts  0.75 us

profile of v3, /device:TPU:0, one launch (start us, length us, event | category | flops | bytes accessed | tf_op | source)
XLA Modules:
  0.0 27.6 jit_solution(6319340434272366175)
XLA Ops:
  0.0 26.9 %shard_map.145 = bf16[1,96,2048]{2,1,0:T(8,128)(2,1)S(1)} custom-call(bf16[1,192,1024]{2,1,0:T(8,128)(2,1)} %tokens.1, bf16[8,128]{1,0:T(8,128)(2,1)} %bitcast.5, bf16[512,512]{1,0:T(8,128)(2,1)} %w_q_down.1, f32[1,512]{1,0:T(1,128)} %bitcast.6, bf16[512,1024]{1,0:T(8,128)(2,1)} %w_q_nope.1, bf16[512,512]{1,0:T(8,128)(2,1)} %w_q_rope.1, ...), custom_call_target="tpu_custom_call" | custom-call | tf_op jit(solution)/shard_map/pallas_call | solution.py:589
  26.9 0.7 %copy.17 = bf16[1,96,2048]{2,1,0:T(8,128)(2,1)} copy(bf16[1,96,2048]{2,1,0:T(8,128)(2,1)S(1)} %shard_map.145) | data formatting | bytes 786432

commit v4 on v3

--- a/solution.py
+++ b/solution.py
@@ -82,7 +82,6 @@
     kcat,
     qcat,
     ctx,
-    att,
     acc,
     share,
     arrived,
@@ -310,8 +309,8 @@
 
     if line:
         spread_word()
-    c_gain.wait()
-    c_tok.wait()
+    c_gain.wait_recv()
+    c_tok.wait_recv()
     whole = jnp.concatenate([tok[0], tok[1]], axis=1).astype(F32)
     lines = gain.shape[1]
     wide_gain = [gain[0].astype(F32), gain[1].astype(F32)]
@@ -352,6 +351,8 @@
     halo_out[1] = pool_in[: 2 * RIM, :].astype(F32)[:RIM, :]
     c_up = remote(halo_out.at[0], halo_in.at[0], SIDE_A, UP, above)
     c_dn = remote(halo_out.at[1], halo_in.at[1], SIDE_B, DOWN, below)
+    c_gain.wait_send()
+    c_tok.wait_send()
     pl.when(has_next)(c_up.start)
     pl.when(has_prev)(c_dn.start)
 
@@ -495,55 +496,83 @@
     spans = length // span_keys
     block = 4 * half
 
-    def attend(part):
-        def one_block(b, carry):
-            block_rows = pl.ds(pl.multiple_of(b * block, block), block)
-            queries = qcat[part, block_rows, :]
-
-            def absorb(keys, state):
-                scores = mm_t(queries, keys)
-                top = jnp.max(scores, axis=1, keepdims=True)
-                if state is not None:
-                    top = jnp.maximum(top, state[0])
-                weights = jnp.exp2((scores - top) * factor)
-                total = jnp.sum(weights, axis=1, keepdims=True)
-                summed = mm(weights.astype(BF16), keys[:, :kv_rank])
-                if state is not None:
-                    shrink = jnp.exp2((state[0] - top) * factor)
-                    total = total + state[1] * shrink
-                    summed = summed + state[2] * shrink
-                return top, total, summed
-
-            if spans == 1:
-                state = absorb(kcat[...], None)
-            else:
-                state = absorb(kcat[:span_keys, :], None)
-
-                def step(i, now):
-                    start = pl.multiple_of(i * span_keys, span_keys)
-                    return absorb(kcat[pl.ds(start, span_keys), :], now)
-
+    @pl.when(q_core)
+    def _():
+        all_taken(kv_lat, n_sp * rows, LATENT)
+
+    kcat[:, :kv_rank] = kv_lat[...]
+
+    def scored(part, first, keys):
+        return mm_t(qcat[part, pl.ds(first, block), :], keys)
+
+    def weighed(scores, keys, state):
+        top = jnp.max(scores, axis=1, keepdims=True)
+        if state is not None:
+            top = jnp.maximum(top, state[0])
+        weights = jnp.exp2((scores - top) * factor)
+        total = jnp.sum(weights, axis=1, keepdims=True)
+        summed = mm(weights.astype(BF16), keys[:, :kv_rank])
+        if state is not None:
+            shrink = jnp.exp2((state[0] - top) * factor)
+            total = total + state[1] * shrink
+            summed = summed + state[2] * shrink
+        return top, total, summed
+
+    part_rows = heads * half
+    blocks = part_rows // block
+
+    def keep(order, index, state):
+        ctx[pl.ds(order * part_rows + index * block, block), :] = (state[2] / state[1]).astype(BF16)
+
+    def projected(order, part):
+        pieces = []
+        for h in range(heads):
+            mixed_latent = ctx[pl.ds(order * part_rows + h * half, half), :]
+            cols = slice(h * VALUE_DIM, (h + 1) * VALUE_DIM)
+            pieces.append(mm(mixed_latent, wvu[:, cols]).astype(BF16))
+        own = acc[pl.ds(pl.multiple_of(part * half, half), half), :]
+        return own + mm(jnp.concatenate(pieces, axis=1), woa[...])
+
+    parts = (1 - t, t)
+    c_share = remote(share, arrived, BLOCK, SHARE, mate)
+
+    def give():
+        share[...] = projected(0, parts[0]).astype(BF16)
+        c_share.start()
+
+    if spans == 1:
+        jobs = [(order, index) for order in range(2) for index in range(blocks)]
+        ahead = scored(parts[0], 0, kcat[...])
+        for i, (order, index) in enumerate(jobs):
+            scores = ahead
+            if i + 1 < len(jobs):
+                later, place_of = jobs[i + 1]
+                ahead = scored(parts[later], place_of * block, kcat[...])
+            keep(order, index, weighed(scores, kcat[...], None))
+            if i == blocks:
+                give()
+    else:
+        for order in range(2):
+
+            def one_block(index, carry):
+                first = pl.multiple_of(index * block, block)
+
+                def step(i, state):
+                    start_key = pl.multiple_of(i * span_keys, span_keys)
+                    keys = kcat[pl.ds(start_key, span_keys), :]
+                    return weighed(scored(parts[order], first, keys), keys, state)
+
+                keys = kcat[:span_keys, :]
+                state = weighed(scored(parts[order], first, keys), keys, None)
                 state = lax.fori_loop(1, spans, step, state)
-            ctx[block_rows, :] = (state[2] / state[1]).astype(BF16)
-            return carry
-
-        lax.fori_loop(0, heads * half // block, one_block, 0, unroll=True)
-        for h in range(heads):
-            cols = slice(h * VALUE_DIM, (h + 1) * VALUE_DIM)
-            att[:, cols] = mm(ctx[h * half : (h + 1) * half, :], wvu[:, cols]).astype(BF16)
-        own = acc[pl.ds(pl.multiple_of(part * half, half), half), :]
-        return own + mm(att[...], woa[...])
-
-
-    @pl.when(q_core)
-    def _():
-        all_taken(kv_lat, n_sp * rows, LATENT)
-
-    kcat[:, :kv_rank] = kv_lat[...]
-    share[...] = attend(1 - t).astype(BF16)
-    c_share = remote(share, arrived, BLOCK, SHARE, mate)
-    c_share.start()
-    mine = attend(t)
+                row = pl.multiple_of(order * part_rows + first, block)
+                ctx[pl.ds(row, block), :] = (state[2] / state[1]).astype(BF16)
+                return carry
+
+            lax.fori_loop(0, blocks, one_block, 0, unroll=True)
+            if order == 0:
+                give()
+    mine = projected(1, parts[1])
     c_share.wait()
     out[0] = (mine + arrived[...].astype(F32)).astype(BF16)
     pl.when(has_next)(c_up.wait_send)
@@ -616,8 +645,7 @@
                 vmem(n_sp, half, 2 * ROPE_DIM),
                 vmem(n_sp * rows, kv_rank + 2 * ROPE_DIM),
                 vmem(2, heads * half, kv_rank + 2 * ROPE_DIM),
-                vmem(heads * half, kv_rank),
-                vmem(half, heads * VALUE_DIM),
+                vmem(2 * heads * half, kv_rank),
                 vmem(rows, d_model, kind=F32),
                 vmem(half, d_model),
                 vmem(half, d_model),

time: 27.8 us -> 27.1 us (0.975)
  Pallas kernels: 26.9 us -> 26.2 us
    pallas_call x1, Pallas kernels: 26.9 us -> 26.2 us  [on_device(): pl.pallas_call(functools.partial(layer, n_sp, n_fs), out_shape=pltpu.VMEM...]
where the time goes in v4:
time: 27.1 us; the launch traced here: 26.9 us
  Pallas kernels  26.2 us (97%)
  local copies, waits for them, and re-layouts  0.75 us (3%)
    pallas_call x1, Pallas kernels, on_device(): pl.pallas_call(functools.partial(layer, n_sp, n_fs), out_shape=pltpu.VMEM...  26.2 us
    unnamed x1, local copies, waits for them, and re-layouts  0.75 us

profile of v4, /device:TPU:0, one launch (start us, length us, event | category | flops | bytes accessed | tf_op | source)
XLA Modules:
  0.0 26.9 jit_solution(14821134061297570260)
XLA Ops:
  0.0 26.2 %shard_map.145 = bf16[1,96,2048]{2,1,0:T(8,128)(2,1)S(1)} custom-call(bf16[1,192,1024]{2,1,0:T(8,128)(2,1)} %tokens.1, bf16[8,128]{1,0:T(8,128)(2,1)} %bitcast.5, bf16[512,512]{1,0:T(8,128)(2,1)} %w_q_down.1, f32[1,512]{1,0:T(1,128)} %bitcast.6, bf16[512,1024]{1,0:T(8,128)(2,1)} %w_q_nope.1, bf16[512,512]{1,0:T(8,128)(2,1)} %w_q_rope.1, ...), custom_call_target="tpu_custom_call" | custom-call | tf_op jit(solution)/shard_map/pallas_call | solution.py:618
  26.2 0.7 %copy.17 = bf16[1,96,2048]{2,1,0:T(8,128)(2,1)} copy(bf16[1,96,2048]{2,1,0:T(8,128)(2,1)S(1)} %shard_map.145) | data formatting | bytes 786432

commit v5 on v4

--- a/solution.py
+++ b/solution.py
@@ -241,17 +241,16 @@
         part = part_of(woa, total // line_bytes)
         pltpu.make_async_copy(part, part, local_sem.at[slot]).wait()
 
-    chunks = 4
-    chunk_rows = depth // chunks
+    sizes = (depth // 4,) * 3 + (depth // 8,) * 2
+    places = tuple(sum(sizes[:turn]) for turn in range(len(sizes)))
+    kv_turns = 2
+    kv_rows = depth // kv_turns
     if hops:
         partners = senders = (near, far)
     else:
         partners = tuple((f + j) % n_fs for j in range(1, n_fs))
         senders = tuple((f + n_fs - j) % n_fs for j in range(1, n_fs))
-    def piece_at(turn):
-        return turn * chunk_rows
-
-    turns = range(chunks)
+    turns = range(len(sizes))
 
     def outgoing(ref, slot, first, size):
         part = down(ref, f, first, size)
@@ -269,19 +268,32 @@
         for copy in copies:
             copy.start()
 
-    kv_out = outgoing(wkv_all, STAGE, 0, depth)
-    q_out = [outgoing(wq_all, STAGE + turn, piece_at(turn), chunk_rows) for turn in turns]
+    kv_out = [
+        outgoing(wkv_all, STAGE + turn, turn * kv_rows, kv_rows) for turn in range(kv_turns)
+    ]
+    q_out = [outgoing(wq_all, STAGE + turn, places[turn], sizes[turn]) for turn in turns]
+    kv_last, q_last = STAGE + kv_turns, STAGE + len(sizes)
     if hops:
-        kv_on = onward(wkv_all, STAGE + 1, 0, depth)
-        last = STAGE + chunks
-        q_on = [onward(wq_all, last, piece_at(turn), chunk_rows) for turn in turns]
+        kv_on = [
+            onward(wkv_all, kv_last, turn * kv_rows, kv_rows) for turn in range(kv_turns)
+        ]
+        q_on = [onward(wq_all, q_last, places[turn], sizes[turn]) for turn in turns]
     else:
-        kv_on = []
+        kv_on = [[] for turn in range(kv_turns)]
         q_on = [[] for turn in turns]
+
+    def from_shard(ref, owner):
+        first = pl.multiple_of(owner * depth, depth)
+        return mm(hid[:, pl.ds(first, depth)], ref[pl.ds(first, depth), :])
+
+    def from_near(ref):
+        return functools.reduce(jnp.add, [from_shard(ref, owner) for owner in (f,) + senders])
+
     @pl.when(kv_core)
     def _():
         l_kv.wait()
-        start(kv_out)
+        for copies in kv_out:
+            start(copies)
 
     l_tok.wait()
     l_gain.wait()
@@ -338,10 +350,15 @@
         here = kv_lat.at[rows_of(owner)]
         return remote(here, here, sent, slot, device)
 
-    base = STAGE + 2
+    base = STAGE + kv_turns + 1
     taken = LATENT
     c_own = latent(s, GATHER, taken, mate)
-    gather_out = [latent(s, GATHER, base + j, {"sp": peer}) for j, peer in enumerate(peers_to)]
+    order_to = list(enumerate(peers_to))
+    if n_sp == 4:
+        high = s // 2
+        edge = 1 - (s + high) % 2
+        order_to = [(1 + edge, 3 - 3 * high), (2 - edge, 2 - high), order_to[0]]
+    gather_out = [latent(s, GATHER, base + j, {"sp": peer}) for j, peer in order_to]
     gather_in = [latent(owner, GATHER, base + j, mate) for j, owner in enumerate(peers_from)]
     passed = [latent(owner, PASS, taken, mate) for owner in peers_from]
 
@@ -375,8 +392,9 @@
 
     @pl.when(kv_core)
     def _():
-        all_taken(wkv_all, len(senders) * depth, STAGE)
-        start(kv_on)
+        for turn in range(kv_turns):
+            all_taken(wkv_all, len(senders) * kv_rows, STAGE + turn)
+            start(kv_on[turn])
 
     def no_rim(side):
         def clear():
@@ -423,16 +441,17 @@
 
     @pl.when(kv_core)
     def _():
+        kv_sum = from_near(wkv_all)
         if hops:
-            all_taken(wkv_all, depth, STAGE + 1)
-        pre = mm(hid[...], wkv_all[...]).astype(BF16).astype(F32)
-        kv_lat[own_rows] = normed(pre, kvg[...])
+            all_taken(wkv_all, depth, kv_last)
+            kv_sum = kv_sum + from_shard(wkv_all, across)
+        kv_lat[own_rows] = normed(kv_sum.astype(BF16).astype(F32), kvg[...])
         start(gather_out + [c_own])
 
     @pl.when(q_core)
     def _():
         for turn in turns:
-            all_taken(wq_all, len(senders) * chunk_rows, STAGE + turn)
+            all_taken(wq_all, len(senders) * sizes[turn], STAGE + turn)
             start(q_on[turn])
 
     def finish_rope(owner):
@@ -449,10 +468,7 @@
         finish_rope(owner)
 
     c_lat = remote(q_lat, q_lat, GATHER, LATENT, mate)
-
-    def from_shard(owner):
-        first = pl.multiple_of(owner * depth, depth)
-        return mm(hid[:, pl.ds(first, depth)], wq_all[pl.ds(first, depth), :])
+    lat_parts = [q_lat.at[pl.ds(part * half, half)] for part in range(2)]
 
     @pl.when(kv_core)
     def _():
@@ -463,14 +479,16 @@
 
     @pl.when(q_core)
     def _():
-        q_part[...] = functools.reduce(jnp.add, [from_shard(owner) for owner in (f,) + senders])
+        q_part[...] = from_near(wq_all)
         if hops:
-            all_taken(wq_all, depth, STAGE + chunks)
+            all_taken(wq_all, depth, q_last)
         q_sum = q_part[...]
         if hops:
-            q_sum = q_sum + from_shard(across)
-        q_lat[...] = normed(q_sum.astype(BF16).astype(F32), qg[...])
-        c_lat.start()
+            q_sum = q_sum + from_shard(wq_all, across)
+        for part, piece in enumerate(lat_parts):
+            some = q_sum[part * half : (part + 1) * half].astype(BF16).astype(F32)
+            piece[...] = normed(some, qg[...])
+            remote(piece, piece, GATHER, LATENT, mate).start()
 
     q_latent = q_lat[...]
     all_loaded(wqn, wqr, wku, wvu)
@@ -524,21 +542,31 @@
     def keep(order, index, state):
         ctx[pl.ds(order * part_rows + index * block, block), :] = (state[2] / state[1]).astype(BF16)
 
-    def projected(order, part):
+    def attended(order):
         pieces = []
         for h in range(heads):
             mixed_latent = ctx[pl.ds(order * part_rows + h * half, half), :]
             cols = slice(h * VALUE_DIM, (h + 1) * VALUE_DIM)
             pieces.append(mm(mixed_latent, wvu[:, cols]).astype(BF16))
-        own = acc[pl.ds(pl.multiple_of(part * half, half), half), :]
-        return own + mm(jnp.concatenate(pieces, axis=1), woa[...])
+        return jnp.concatenate(pieces, axis=1)
+
+    def projected(features, part, side):
+        cols = slice(side * side_width, (side + 1) * side_width)
+        own = acc[pl.ds(pl.multiple_of(part * half, half), half), cols]
+        return own + mm(features, woa[:, cols])
 
     parts = (1 - t, t)
+    side_width = share.shape[2]
+    shares = [
+        remote(share.at[side], arrived.at[side], BLOCK, SHARE, mate) for side in range(2)
+    ]
     c_share = remote(share, arrived, BLOCK, SHARE, mate)
 
     def give():
-        share[...] = projected(0, parts[0]).astype(BF16)
-        c_share.start()
+        features = attended(0)
+        for side in range(2):
+            share[side] = projected(features, parts[0], side).astype(BF16)
+            shares[side].start()
 
     if spans == 1:
         jobs = [(order, index) for order in range(2) for index in range(blocks)]
@@ -572,9 +600,12 @@
             lax.fori_loop(0, blocks, one_block, 0, unroll=True)
             if order == 0:
                 give()
-    mine = projected(1, parts[1])
+    features = attended(1)
+    mine = [projected(features, parts[1], side) for side in range(2)]
     c_share.wait()
-    out[0] = (mine + arrived[...].astype(F32)).astype(BF16)
+    for side in range(2):
+        cols = slice(side * side_width, (side + 1) * side_width)
+        out[0, :, cols] = (mine[side] + arrived[side].astype(F32)).astype(BF16)
     pl.when(has_next)(c_up.wait_send)
     pl.when(has_prev)(c_dn.wait_send)
 
@@ -647,11 +678,11 @@
                 vmem(2, heads * half, kv_rank + 2 * ROPE_DIM),
                 vmem(2 * heads * half, kv_rank),
                 vmem(rows, d_model, kind=F32),
-                vmem(half, d_model),
-                vmem(half, d_model),
+                vmem(2, half, d_model // 2),
+                vmem(2, half, d_model // 2),
                 dma((9,)),
                 dma((6,)),
-                dma((STAGE + max(5, n_sp + 1),)),
+                dma((STAGE + max(6, n_sp + 2),)),
                 pltpu.SemaphoreType.REGULAR((2,)),
             ],
             compiler_params=pltpu.CompilerParams(collective_id=0, has_side_effects=True, vmem_limit_bytes=40 * 1024 * 1024),

time: 27.1 us -> 26 us (0.959)
  Pallas kernels: 26.2 us -> 25.1 us
    pallas_call x1, Pallas kernels: 26.2 us -> 25.1 us  [on_device(): pl.pallas_call(functools.partial(layer, n_sp, n_fs), out_shape=pltpu.VMEM...]
where the time goes in v5:
time: 26 us; the launch traced here: 25.8 us
  Pallas kernels  25.1 us (97%)
  local copies, waits for them, and re-layouts  0.75 us (3%)
    pallas_call x1, Pallas kernels, on_device(): pl.pallas_call(functools.partial(layer, n_sp, n_fs), out_shape=pltpu.VMEM...  25.1 us
    unnamed x1, local copies, waits for them, and re-layouts  0.75 us

profile of v5, /device:TPU:0, one launch (start us, length us, event | category | flops | bytes accessed | tf_op | source)
XLA Modules:
  0.0 25.8 jit_solution(2263659492342401392)
XLA Ops:
  0.0 25.1 %shard_map.145 = bf16[1,96,2048]{2,1,0:T(8,128)(2,1)S(1)} custom-call(bf16[1,192,1024]{2,1,0:T(8,128)(2,1)} %tokens.1, bf16[8,128]{1,0:T(8,128)(2,1)} %bitcast.5, bf16[512,512]{1,0:T(8,128)(2,1)} %w_q_down.1, f32[1,512]{1,0:T(1,128)} %bitcast.6, bf16[512,1024]{1,0:T(8,128)(2,1)} %w_q_nope.1, bf16[512,512]{1,0:T(8,128)(2,1)} %w_q_rope.1, ...), custom_call_target="tpu_custom_call" | custom-call | tf_op jit(solution)/shard_map/pallas_call | solution.py:649
  25.1 0.7 %copy.17 = bf16[1,96,2048]{2,1,0:T(8,128)(2,1)} copy(bf16[1,96,2048]{2,1,0:T(8,128)(2,1)S(1)} %shard_map.145) | data formatting | bytes 786432

commit v6 on v5

--- a/solution.py
+++ b/solution.py
@@ -76,6 +76,7 @@
     halo_out,
     halo_in,
     q_part,
+    q_first,
     q_lat,
     kv_lat,
     ropes,
@@ -256,12 +257,12 @@
         part = down(ref, f, first, size)
         return [remote(part, part, MAIN, slot, {"fs": peer}) for peer in partners]
 
-    def onward(ref, slot, first, size):
+    def onward(ref, slot, first, size, core):
         piece = size // 2
         low, high = down(ref, near, first, piece), down(ref, far, first + piece, piece)
         return [
-            remote(low, low, MAIN, slot, {"fs": far}),
-            remote(high, high, MAIN, slot, {"fs": near}),
+            remote(low, low, MAIN, slot, {"fs": far, "tp": core}),
+            remote(high, high, MAIN, slot, {"fs": near, "tp": core}),
         ]
 
     def start(copies):
@@ -272,12 +273,13 @@
         outgoing(wkv_all, STAGE + turn, turn * kv_rows, kv_rows) for turn in range(kv_turns)
     ]
     q_out = [outgoing(wq_all, STAGE + turn, places[turn], sizes[turn]) for turn in turns]
-    kv_last, q_last = STAGE + kv_turns, STAGE + len(sizes)
+    kv_last, lat_slot = STAGE + kv_turns, STAGE + len(sizes)
+    q_last = STAGE + max(len(sizes) + 1, kv_turns + n_sp)
     if hops:
         kv_on = [
-            onward(wkv_all, kv_last, turn * kv_rows, kv_rows) for turn in range(kv_turns)
+            onward(wkv_all, kv_last, turn * kv_rows, kv_rows, t) for turn in range(kv_turns)
         ]
-        q_on = [onward(wq_all, q_last, places[turn], sizes[turn]) for turn in turns]
+        q_on = [onward(wq_all, q_last, places[turn], sizes[turn], 1 - t) for turn in turns]
     else:
         kv_on = [[] for turn in range(kv_turns)]
         q_on = [[] for turn in turns]
@@ -436,6 +438,8 @@
         mean = (mm(band.astype(BF16), padded[:, cols]) / count).astype(BF16)
         spread = (mean.astype(F32) - pool_in[:, cols].astype(F32)).astype(BF16)
         pooled.append(mm(spread, mix[g]).astype(BF16))
+    pl.when(has_next)(c_up.wait_send)
+    pl.when(has_prev)(c_dn.wait_send)
     acc[...] = mm(jnp.concatenate(pooled, axis=1), wop[...])
 
 
@@ -467,28 +471,35 @@
     for owner in (s,) + peers_from:
         finish_rope(owner)
 
-    c_lat = remote(q_lat, q_lat, GATHER, LATENT, mate)
+    c_first = remote(q_part, q_first, GATHER, LATENT, mate)
+    c_lat = remote(q_lat, q_lat, SIDE_A, lat_slot, mate)
     lat_parts = [q_lat.at[pl.ds(part * half, half)] for part in range(2)]
 
+    def pass_on(j):
+        gather_in[j].wait_recv()
+        passed[j].start()
+
     @pl.when(kv_core)
     def _():
-        for j in range(n_sp - 1):
-            gather_in[j].wait_recv()
-            passed[j].start()
-        c_lat.wait_recv()
-
-    @pl.when(q_core)
-    def _():
-        q_part[...] = from_near(wq_all)
+        for j in range(n_sp - 3):
+            pass_on(j)
+        c_first.wait_recv()
+        q_sum = q_first[...]
         if hops:
             all_taken(wq_all, depth, q_last)
-        q_sum = q_part[...]
-        if hops:
             q_sum = q_sum + from_shard(wq_all, across)
         for part, piece in enumerate(lat_parts):
             some = q_sum[part * half : (part + 1) * half].astype(BF16).astype(F32)
             piece[...] = normed(some, qg[...])
-            remote(piece, piece, GATHER, LATENT, mate).start()
+            remote(piece, piece, SIDE_A, lat_slot, mate).start()
+        for j in range(n_sp - 3, n_sp - 1):
+            pass_on(j)
+
+    @pl.when(q_core)
+    def _():
+        q_part[...] = from_near(wq_all)
+        c_first.start()
+        c_lat.wait_recv()
 
     q_latent = q_lat[...]
     all_loaded(wqn, wqr, wku, wvu)
@@ -550,23 +561,16 @@
             pieces.append(mm(mixed_latent, wvu[:, cols]).astype(BF16))
         return jnp.concatenate(pieces, axis=1)
 
-    def projected(features, part, side):
-        cols = slice(side * side_width, (side + 1) * side_width)
-        own = acc[pl.ds(pl.multiple_of(part * half, half), half), cols]
-        return own + mm(features, woa[:, cols])
+    def projected(features, part):
+        own = acc[pl.ds(pl.multiple_of(part * half, half), half), :]
+        return own + mm(features, woa[...])
 
     parts = (1 - t, t)
-    side_width = share.shape[2]
-    shares = [
-        remote(share.at[side], arrived.at[side], BLOCK, SHARE, mate) for side in range(2)
-    ]
     c_share = remote(share, arrived, BLOCK, SHARE, mate)
 
     def give():
-        features = attended(0)
-        for side in range(2):
-            share[side] = projected(features, parts[0], side).astype(BF16)
-            shares[side].start()
+        share[...] = projected(attended(0), parts[0]).astype(BF16)
+        c_share.start()
 
     if spans == 1:
         jobs = [(order, index) for order in range(2) for index in range(blocks)]
@@ -600,25 +604,21 @@
             lax.fori_loop(0, blocks, one_block, 0, unroll=True)
             if order == 0:
                 give()
-    features = attended(1)
-    mine = [projected(features, parts[1], side) for side in range(2)]
+    mine = projected(attended(1), parts[1])
     c_share.wait()
-    for side in range(2):
-        cols = slice(side * side_width, (side + 1) * side_width)
-        out[0, :, cols] = (mine[side] + arrived[side].astype(F32)).astype(BF16)
-    pl.when(has_next)(c_up.wait_send)
-    pl.when(has_prev)(c_dn.wait_send)
+    out[0] = (mine + arrived[...].astype(F32)).astype(BF16)
 
     @pl.when(kv_core)
     def _():
         all_sent(wkv_all, (n_fs - 1) * depth, MAIN)
         all_sent(kv_lat, n_sp * rows, GATHER)
         all_sent(kv_lat, (n_sp - 1) * rows, PASS)
+        c_lat.wait_send()
 
     @pl.when(q_core)
     def _():
         all_sent(wq_all, (n_fs - 1) * depth, MAIN)
-        c_lat.wait_send()
+        c_first.wait_send()
 
 
 def solution(mesh):
@@ -671,6 +671,7 @@
                 vmem(2, RIM, wpi.shape[1], kind=F32),
                 vmem(2, RIM, wpi.shape[1], kind=F32),
                 vmem(rows, q_rank, kind=F32),
+                vmem(rows, q_rank, kind=F32),
                 vmem(rows, q_rank),
                 vmem(n_sp * rows, kv_rank),
                 vmem(n_sp, half, 2 * ROPE_DIM),
@@ -678,11 +679,11 @@
                 vmem(2, heads * half, kv_rank + 2 * ROPE_DIM),
                 vmem(2 * heads * half, kv_rank),
                 vmem(rows, d_model, kind=F32),
-                vmem(2, half, d_model // 2),
-                vmem(2, half, d_model // 2),
+                vmem(half, d_model),
+                vmem(half, d_model),
                 dma((9,)),
                 dma((6,)),
-                dma((STAGE + max(6, n_sp + 2),)),
+                dma((STAGE + max(6, n_sp + 2) + 1,)),
                 pltpu.SemaphoreType.REGULAR((2,)),
             ],
             compiler_params=pltpu.CompilerParams(collective_id=0, has_side_effects=True, vmem_limit_bytes=40 * 1024 * 1024),

time: 26 us -> 25.5 us (0.981)
  Pallas kernels: 25.1 us -> 24.6 us
    pallas_call x1, Pallas kernels: 25.1 us -> 24.6 us  [on_device(): pl.pallas_call(functools.partial(layer, n_sp, n_fs), out_shape=pltpu.VMEM...]
where the time goes in v6:
time: 25.5 us; the launch traced here: 25.4 us
  Pallas kernels  24.6 us (96%)
  local copies, waits for them, and re-layouts  0.75 us (3%)
    pallas_call x1, Pallas kernels, on_device(): pl.pallas_call(functools.partial(layer, n_sp, n_fs), out_shape=pltpu.VMEM...  24.6 us
    unnamed x1, local copies, waits for them, and re-layouts  0.75 us

profile of v6, /device:TPU:0, one launch (start us, length us, event | category | flops | bytes accessed | tf_op | source)
XLA Modules:
  0.0 25.4 jit_solution(6443671874805281238)
XLA Ops:
  0.0 24.6 %shard_map.145 = bf16[1,96,2048]{2,1,0:T(8,128)(2,1)S(1)} custom-call(bf16[1,192,1024]{2,1,0:T(8,128)(2,1)} %tokens.1, bf16[8,128]{1,0:T(8,128)(2,1)} %bitcast.5, bf16[512,512]{1,0:T(8,128)(2,1)} %w_q_down.1, f32[1,512]{1,0:T(1,128)} %bitcast.6, bf16[512,1024]{1,0:T(8,128)(2,1)} %w_q_nope.1, bf16[512,512]{1,0:T(8,128)(2,1)} %w_q_rope.1, ...), custom_call_target="tpu_custom_call" | custom-call | tf_op jit(solution)/shard_map/pallas_call | solution.py:649
  24.6 0.7 %copy.17 = bf16[1,96,2048]{2,1,0:T(8,128)(2,1)} copy(bf16[1,96,2048]{2,1,0:T(8,128)(2,1)S(1)} %shard_map.145) | data formatting | bytes 786432

commit v7 on v6

--- a/solution.py
+++ b/solution.py
@@ -242,7 +242,7 @@
         part = part_of(woa, total // line_bytes)
         pltpu.make_async_copy(part, part, local_sem.at[slot]).wait()
 
-    sizes = (depth // 4,) * 3 + (depth // 8,) * 2
+    sizes = (depth // 4,) * 3 + (depth // 8, depth // 16, depth // 16)
     places = tuple(sum(sizes[:turn]) for turn in range(len(sizes)))
     kv_turns = 2
     kv_rows = depth // kv_turns
@@ -279,14 +279,17 @@
         kv_on = [
             onward(wkv_all, kv_last, turn * kv_rows, kv_rows, t) for turn in range(kv_turns)
         ]
-        q_on = [onward(wq_all, q_last, places[turn], sizes[turn], 1 - t) for turn in turns]
+        q_on = [
+            onward(wq_all, q_last + turn // 3, places[turn], sizes[turn], 1 - t)
+            for turn in turns
+        ]
     else:
         kv_on = [[] for turn in range(kv_turns)]
         q_on = [[] for turn in turns]
 
-    def from_shard(ref, owner):
-        first = pl.multiple_of(owner * depth, depth)
-        return mm(hid[:, pl.ds(first, depth)], ref[pl.ds(first, depth), :])
+    def from_shard(ref, owner, at=0, size=depth):
+        first = pl.multiple_of(owner * depth + at, 128)
+        return mm(hid[:, pl.ds(first, size)], ref[pl.ds(first, size), :])
 
     def from_near(ref):
         return functools.reduce(jnp.add, [from_shard(ref, owner) for owner in (f,) + senders])
@@ -486,8 +489,11 @@
         c_first.wait_recv()
         q_sum = q_first[...]
         if hops:
-            all_taken(wq_all, depth, q_last)
-            q_sum = q_sum + from_shard(wq_all, across)
+            early = sum(sizes[:3])
+            all_taken(wq_all, early, q_last)
+            q_sum = q_sum + from_shard(wq_all, across, 0, early)
+            all_taken(wq_all, depth - early, q_last + 1)
+            q_sum = q_sum + from_shard(wq_all, across, early, depth - early)
         for part, piece in enumerate(lat_parts):
             some = q_sum[part * half : (part + 1) * half].astype(BF16).astype(F32)
             piece[...] = normed(some, qg[...])
@@ -683,7 +689,7 @@
                 vmem(half, d_model),
                 dma((9,)),
                 dma((6,)),
-                dma((STAGE + max(6, n_sp + 2) + 1,)),
+                dma((STAGE + max(7, n_sp + 2) + 2,)),
                 pltpu.SemaphoreType.REGULAR((2,)),
             ],
             compiler_params=pltpu.CompilerParams(collective_id=0, has_side_effects=True, vmem_limit_bytes=40 * 1024 * 1024),

time: 25.5 us -> 25.3 us (level)
  no operation moved by 1% of the time
where the time goes in v7:
time: 25.3 us; the launch traced here: 25.1 us
  Pallas kernels  24.4 us (96%)
  local copies, waits for them, and re-layouts  0.75 us (3%)
    pallas_call x1, Pallas kernels, on_device(): pl.pallas_call(functools.partial(layer, n_sp, n_fs), out_shape=pltpu.VMEM...  24.4 us
    unnamed x1, local copies, waits for them, and re-layouts  0.75 us

profile of v7, /device:TPU:0, one launch (start us, length us, event | category | flops | bytes accessed | tf_op | source)
XLA Modules:
  0.0 25.1 jit_solution(13982023365873156690)
XLA Ops:
  0.0 24.4 %shard_map.145 = bf16[1,96,2048]{2,1,0:T(8,128)(2,1)S(1)} custom-call(bf16[1,192,1024]{2,1,0:T(8,128)(2,1)} %tokens.1, bf16[8,128]{1,0:T(8,128)(2,1)} %bitcast.5, bf16[512,512]{1,0:T(8,128)(2,1)} %w_q_down.1, f32[1,512]{1,0:T(1,128)} %bitcast.6, bf16[512,1024]{1,0:T(8,128)(2,1)} %w_q_nope.1, bf16[512,512]{1,0:T(8,128)(2,1)} %w_q_rope.1, ...), custom_call_target="tpu_custom_call" | custom-call | tf_op jit(solution)/shard_map/pallas_call | solution.py:655
  24.4 0.7 %copy.17 = bf16[1,96,2048]{2,1,0:T(8,128)(2,1)} copy(bf16[1,96,2048]{2,1,0:T(8,128)(2,1)S(1)} %shard_map.145) | data formatting | bytes 786432

commit v8 on v7

--- a/solution.py
+++ b/solution.py
@@ -146,7 +146,8 @@
         l_vu,
         l_oa,
     ) = loads
-    for load in loads:
+    first_loads, later_loads = loads[:8], loads[8:]
+    for load in first_loads:
         if load is l_kv:
             pl.when(kv_core)(load.start)
         elif load is l_q:
@@ -306,6 +307,8 @@
     c_tok.start()
     c_gain = remote(gain.at[t], gain.at[t], SIDE_B, GAIN, mate)
     c_gain.start()
+    for load in later_loads:
+        load.start()
     lane = lax.broadcasted_iota(jnp.int32, (rows, 128), 1)
     place = s * rows + lax.broadcasted_iota(jnp.int32, (rows, 128), 0)
     quarter = ROPE_DIM // 4

time: 25.3 us -> 25.3 us (level)
  no operation moved by 1% of the time
where the time goes in v8:
time: 25.3 us; the launch traced here: 25.1 us
  Pallas kernels  24.4 us (96%)
  local copies, waits for them, and re-layouts  0.75 us (3%)
    pallas_call x1, Pallas kernels, on_device(): pl.pallas_call(functools.partial(layer, n_sp, n_fs), out_shape=pltpu.VMEM...  24.4 us
    unnamed x1, local copies, waits for them, and re-layouts  0.75 us

profile of v8, /device:TPU:0, one launch (start us, length us, event | category | flops | bytes accessed | tf_op | source)
XLA Modules:
  0.0 25.1 jit_solution(14281315708321723499)
XLA Ops:
  0.0 24.4 %shard_map.145 = bf16[1,96,2048]{2,1,0:T(8,128)(2,1)S(1)} custom-call(bf16[1,192,1024]{2,1,0:T(8,128)(2,1)} %tokens.1, bf16[8,128]{1,0:T(8,128)(2,1)} %bitcast.5, bf16[512,512]{1,0:T(8,128)(2,1)} %w_q_down.1, f32[1,512]{1,0:T(1,128)} %bitcast.6, bf16[512,1024]{1,0:T(8,128)(2,1)} %w_q_nope.1, bf16[512,512]{1,0:T(8,128)(2,1)} %w_q_rope.1, ...), custom_call_target="tpu_custom_call" | custom-call | tf_op jit(solution)/shard_map/pallas_call | solution.py:658
  24.4 0.7 %copy.17 = bf16[1,96,2048]{2,1,0:T(8,128)(2,1)} copy(bf16[1,96,2048]{2,1,0:T(8,128)(2,1)S(1)} %shard_map.145) | data formatting | bytes 786432
